TPU v7x, 32 devices: a whole 2x2x4 slice. The times are simulated.
32 devices in a mesh: sp: 4 (over z), fs: 4 (over y, x), tp: 2 (over core).
Axes of the slice: x: 2, y: 2, z: 4, core: 2. Of those that a mesh axis runs over, the one named last changes fastest.
Arguments:
- tokens: bfloat16 [8192, 2048], P(('fs', 'sp')), parts along dimension 0, may hold values from -6 to 6
- norm_gain: float32 [2048], replicated, may hold values from 0.1 to 1.9
- state_gate: bfloat16 [2048, 1024], P('sp', 'tp'), may hold values from -0.125 to 0.125
- state_value: bfloat16 [2048, 1024], P('sp', 'tp'), may hold values from -0.125 to 0.125
- state_keys: bfloat16 [2048, 1024], P('sp', 'tp'), may hold values from -0.125 to 0.125
- state_query: bfloat16 [2048, 1024], P('sp', 'tp'), may hold values from -0.125 to 0.125
- state_step: bfloat16 [2048, 16], replicated, may hold values from -0.125 to 0.125
- state_rate: float32 [16], P('tp'), may hold values from 0 to 1, as said below
- state_jumps: float32 [8192, 16], P(('fs', 'sp'), 'tp'), parts along dimension 0, may hold values from -3 to 0
- state_gain: float32 [1024], P('tp'), may hold values from 0.1 to 1.9
- filter_value: bfloat16 [5, 1024], P(None, 'tp'), may hold values from -2.5 to 2.5
- filter_keys: bfloat16 [5, 1024], P(None, 'tp'), may hold values from -2.5 to 2.5
- filter_query: bfloat16 [5, 1024], P(None, 'tp'), may hold values from -2.5 to 2.5
- window_query: bfloat16 [2048, 2048], P('sp', 'tp'), may hold values from -64 to 64
- window_keys: bfloat16 [2048, 1024], P('sp', 'tp'), may hold values from -1 to 1
- window_values: bfloat16 [2048, 1024], P('sp', 'tp'), may hold values from -0.125 to 0.125
- window_sink: float32 [16], P('tp'), may hold values from 2.5 to 5.5
- state_output: bfloat16 [1024, 2048], P('tp', 'sp'), may hold values from -0.1875 to 0.1875
- window_output: bfloat16 [2048, 2048], P('tp', 'sp'), may hold values from -2 to 2
Outputs:
- mixed: bfloat16 [8192, 2048], P(('fs', 'sp', 'tp')), parts along dimension 0
There are 4 independent parts, one for each index of `fs`. A program takes and returns all parts, laid end to end along the dimension named above; an argument that names none is the same for every part. Nothing has to cross between parts.
Inputs may be any that keep to these rules, and one draw needn't show every extreme that they name: `state_rate`: a positive rate for each head.
All inputs are finite; a program needn't handle non-finite values.
Results may differ from a plain program's by a relative error of at most 0.015.
The roundings to bfloat16 on the way count: a program that leaves them out, or rounds other values in their place, can miss the bound.
Values may be sent and summed in bfloat16 or wider, within the bound.
A program may use at most 64 MiB of HBM per device.

v0:
```python
import functools
import math

import jax
import jax.numpy as jnp
from jax import lax
from jax.experimental import pallas as pl
from jax.experimental.pallas import tpu as pltpu
from jax.sharding import PartitionSpec as P

STATE_SIZE = 128
HEAD_DIM = 128
WINDOW = 128
BLOCK = 128
GRID_WIDTH = 64


def extended(cells, sides, width):
    for axis, dim in sides:
        count = lax.axis_size(axis)
        ends = count - 1
        head = lax.slice_in_dim(cells, 0, width, axis=dim)
        tail = lax.slice_in_dim(cells, cells.shape[dim] - width, cells.shape[dim], axis=dim)
        cells = jnp.concatenate(
            [
                lax.ppermute(tail, axis, [(i, (i + 1) % count) for i in range(ends)]),
                cells,
                lax.ppermute(head, axis, [((i + 1) % count, i) for i in range(ends)]),
            ],
            axis=dim,
        )
    return cells


def rotate_grid(vectors, positions, grid_width):
    head_dim = vectors.shape[-1]
    quarter = head_dim // 4
    half_dim = head_dim // 2
    inverse = 10000.0 ** (-jnp.arange(quarter, dtype=jnp.float32) / quarter)
    grid_row = (positions // grid_width).astype(jnp.float32)
    grid_col = (positions % grid_width).astype(jnp.float32)
    angle_row = grid_row[:, None] * inverse[None, :]
    angle_col = grid_col[:, None] * inverse[None, :]
    angles = jnp.concatenate([angle_row, angle_row, angle_col, angle_col], axis=-1)[:, None, :]
    first_half = vectors[..., :half_dim]
    second = vectors[..., half_dim:]
    turned = jnp.concatenate(
        [
            -first_half[..., quarter:],
            first_half[..., :quarter],
            -second[..., quarter:],
            second[..., :quarter],
        ],
        axis=-1,
    )
    return (
        vectors.astype(jnp.float32) * jnp.cos(angles) + turned.astype(jnp.float32) * jnp.sin(angles)
    ).astype(jnp.bfloat16)


def window_attend(query_rows, keys_pad, values_pad, sink_logits, key_start, total_len, window):
    row_count, query_heads, head_dim = query_rows.shape
    kv_heads = keys_pad.shape[1]
    group_size = query_heads // kv_heads
    block_count = row_count // window
    query_blocks = query_rows.reshape(block_count, window, kv_heads, group_size, head_dim)
    key_split = keys_pad.reshape(block_count + 2, window, kv_heads, head_dim)
    value_split = values_pad.reshape(block_count + 2, window, kv_heads, head_dim)
    key_band = jnp.concatenate([key_split[:-2], key_split[1:-1], key_split[2:]], axis=1)
    value_band = jnp.concatenate([value_split[:-2], value_split[1:-1], value_split[2:]], axis=1)
    scores = jnp.einsum(
        "kihgd,kjhd->khgij", query_blocks, key_band, preferred_element_type=jnp.float32
    ) * head_dim ** (-0.5)
    query_pos = jnp.arange(window)[:, None]
    band_pos = jnp.arange(3 * window)[None, :]
    within = jnp.abs(band_pos - window - query_pos) <= window
    key_pos = (
        key_start + jnp.arange(block_count)[:, None] * window + jnp.arange(3 * window)[None, :]
    )
    inside = (key_pos >= 0) & (key_pos < total_len)
    valid_pair = (within[None] & inside[:, None, :])[:, None, None]
    sink_logit = sink_logits.reshape(kv_heads, group_size)[None, :, :, None, None]
    masked = jnp.where(valid_pair, scores, -1e30)
    ceiling = jnp.maximum(jnp.max(masked, axis=-1, keepdims=True), sink_logit)
    weights = jnp.where(valid_pair, jnp.exp(masked - ceiling), 0.0)
    denominator = jnp.exp(sink_logit - ceiling) + jnp.sum(weights, axis=-1, keepdims=True)
    weights_bf = (weights / denominator).astype(jnp.bfloat16)
    mixed_rows = jnp.einsum(
        "khgij,kjhd->kihgd", weights_bf, value_band, preferred_element_type=jnp.float32
    )
    return mixed_rows.reshape(row_count, query_heads * head_dim).astype(jnp.bfloat16)


def block_terms(query_rows, key_rows, value_rows, log_rows, block_len):
    row_count, group_count, state_size = query_rows.shape
    head_ratio, head_dim = (value_rows.shape[2], value_rows.shape[3])
    block_count = row_count // block_len
    query_blocks = query_rows.reshape(block_count, block_len, group_count, state_size)
    key_blocks = key_rows.reshape(block_count, block_len, group_count, state_size)
    value_blocks = value_rows.reshape(block_count, block_len, group_count, head_ratio, head_dim)
    decay_cum = jnp.cumsum(
        log_rows.reshape(block_count, block_len, group_count, head_ratio), axis=1
    )
    decay_total = decay_cum[:, -1]
    gram_block = jnp.einsum(
        "kign,kjgn->kgij", query_blocks, key_blocks, preferred_element_type=jnp.float32
    )
    cum_heads = jnp.moveaxis(decay_cum, 1, 3)
    distance = jnp.abs(cum_heads[..., :, None] - cum_heads[..., None, :])
    pair_weight = (gram_block[:, :, None] * jnp.exp(-distance)).astype(jnp.bfloat16)
    near_terms = jnp.einsum(
        "kgrij,kjgrp->kigrp", pair_weight, value_blocks, preferred_element_type=jnp.float32
    )
    keys_after = (
        key_blocks[:, :, :, None, :] * jnp.exp(decay_total[:, None] - decay_cum)[..., None]
    ).astype(jnp.bfloat16)
    keys_before = (key_blocks[:, :, :, None, :] * jnp.exp(decay_cum)[..., None]).astype(
        jnp.bfloat16
    )
    state_after = jnp.einsum(
        "kjgrn,kjgrp->kgrnp", keys_after, value_blocks, preferred_element_type=jnp.float32
    )
    state_before = jnp.einsum(
        "kjgrn,kjgrp->kgrnp", keys_before, value_blocks, preferred_element_type=jnp.float32
    )
    before = jnp.cumsum(decay_total, axis=0) - decay_total
    overall = jnp.sum(decay_total, axis=0)
    after_sum = overall[None] - before - decay_total
    block_order = jnp.arange(block_count)
    earlier_mask = (block_order[None, :] < block_order[:, None])[:, :, None, None]
    later_mask = (block_order[None, :] > block_order[:, None])[:, :, None, None]
    gap_fwd = before[:, None] - before[None, :] - decay_total[None, :]
    gap_bwd = before[None, :] - before[:, None] - decay_total[:, None]
    weight_fwd = jnp.where(earlier_mask, jnp.exp(jnp.minimum(gap_fwd, 0.0)), 0.0)
    weight_bwd = jnp.where(later_mask, jnp.exp(jnp.minimum(gap_bwd, 0.0)), 0.0)
    carried_fwd = jnp.einsum(
        "abgr,bgrnp->agrnp", weight_fwd, state_after, precision=lax.Precision.HIGHEST
    )
    carried_bwd = jnp.einsum(
        "abgr,bgrnp->agrnp", weight_bwd, state_before, precision=lax.Precision.HIGHEST
    )
    summary_fwd = jnp.einsum(
        "agr,agrnp->grnp", jnp.exp(after_sum), state_after, precision=lax.Precision.HIGHEST
    )
    summary_bwd = jnp.einsum(
        "agr,agrnp->grnp", jnp.exp(before), state_before, precision=lax.Precision.HIGHEST
    )
    pieces = (
        near_terms,
        carried_fwd,
        carried_bwd,
        decay_cum,
        decay_total,
        before,
        after_sum,
        query_blocks,
    )
    return (pieces, (summary_fwd, summary_bwd, overall))


def finish_terms(pieces, incoming_fwd, incoming_bwd):
    (
        near_terms,
        carried_fwd,
        carried_bwd,
        decay_cum,
        decay_total,
        before,
        after_sum,
        query_blocks,
    ) = pieces
    total_fwd = carried_fwd + jnp.exp(before)[..., None, None] * incoming_fwd[None]
    total_bwd = carried_bwd + jnp.exp(after_sum)[..., None, None] * incoming_bwd[None]
    query_wide = query_blocks.astype(jnp.float32)
    read_fwd = jnp.einsum(
        "kign,kgrnp->kigrp", query_wide, total_fwd, precision=lax.Precision.HIGHEST
    )
    read_bwd = jnp.einsum(
        "kign,kgrnp->kigrp", query_wide, total_bwd, precision=lax.Precision.HIGHEST
    )
    combined = (
        near_terms
        + jnp.exp(decay_cum)[..., None] * read_fwd
        + jnp.exp(decay_total[:, None] - decay_cum)[..., None] * read_bwd
    )
    block_count, block_len, group_count, head_ratio, head_dim = combined.shape
    return combined.reshape(block_count * block_len, group_count, head_ratio, head_dim)


def combine_all(gathered_states, own_index):
    after_all, before_all, logs_all = gathered_states
    device_count = logs_all.shape[0]
    cum_incl = jnp.cumsum(logs_all, axis=0)
    cum_excl = cum_incl - logs_all
    device_order = jnp.arange(device_count)
    picker = (device_order == own_index).astype(jnp.float32)[:, None, None]
    own_incl = jnp.sum(picker * cum_incl, axis=0)
    own_excl = jnp.sum(picker * cum_excl, axis=0)
    lower_mask = (device_order < own_index)[:, None, None]
    higher_mask = (device_order > own_index)[:, None, None]
    weight_fwd = jnp.where(lower_mask, jnp.exp(jnp.minimum(own_excl[None] - cum_incl, 0.0)), 0.0)
    weight_bwd = jnp.where(higher_mask, jnp.exp(jnp.minimum(cum_excl - own_incl[None], 0.0)), 0.0)
    incoming_fwd = jnp.einsum(
        "dgr,dgrnp->grnp", weight_fwd, after_all, precision=lax.Precision.HIGHEST
    )
    incoming_bwd = jnp.einsum(
        "dgr,dgrnp->grnp", weight_bwd, before_all, precision=lax.Precision.HIGHEST
    )
    return (incoming_fwd, incoming_bwd)


def shards(
    tokens,
    norm_gain,
    state_gate,
    state_value,
    state_keys,
    state_query,
    state_step,
    state_rate,
    state_jumps,
    state_gain,
    filter_value,
    filter_keys,
    filter_query,
    window_query,
    window_keys,
    window_values,
    window_sink,
    state_output,
    window_output,
):
    row_count = tokens.shape[0]
    rows_wide = tokens.astype(jnp.float32)
    normed = (
        rows_wide
        * lax.rsqrt(jnp.mean(rows_wide * rows_wide, axis=-1, keepdims=True) + 1e-06)
        * norm_gain
    ).astype(jnp.bfloat16)
    gathered = (
        lax.all_gather(state_gate, "sp", axis=0, tiled=True),
        lax.all_gather(state_value, "sp", axis=0, tiled=True),
        lax.all_gather(state_keys, "sp", axis=0, tiled=True),
        lax.all_gather(state_query, "sp", axis=0, tiled=True),
        lax.all_gather(window_query, "sp", axis=0, tiled=True),
        lax.all_gather(window_keys, "sp", axis=0, tiled=True),
        lax.all_gather(window_values, "sp", axis=0, tiled=True),
        lax.all_gather(state_output, "sp", axis=1, tiled=True),
        lax.all_gather(window_output, "sp", axis=1, tiled=True),
    )
    projected = [
        jnp.dot(normed, matrix, preferred_element_type=jnp.float32) for matrix in gathered[:7]
    ]
    out_state = gathered[7]
    out_window = gathered[8]
    gate_rows, value_pre, keys_pre, query_pre, query_raw, keys_raw, values_rows = [
        result.astype(jnp.bfloat16) for result in projected
    ]
    head_local = state_rate.shape[0]
    group_local = keys_pre.shape[1] // STATE_SIZE
    head_dim = value_pre.shape[1] // head_local
    head_ratio = head_local // group_local
    step_cols = lax.dynamic_slice_in_dim(
        state_step, lax.axis_index("tp") * head_local, head_local, 1
    )
    step_rows = jax.nn.softplus(jnp.dot(normed, step_cols, preferred_element_type=jnp.float32))
    log_decay = -state_rate[None, :] * step_rows + state_jumps
    half_width = filter_value.shape[0] // 2
    stacked = jnp.concatenate([value_pre, keys_pre, query_pre], axis=-1)
    padded = extended(stacked, (("sp", 0),), half_width)
    filters = jnp.concatenate([filter_value, filter_keys, filter_query], axis=-1).astype(
        jnp.float32
    )
    filtered = jnp.zeros(stacked.shape, jnp.float32)
    for offset in range(filters.shape[0]):
        filtered = (
            filtered + padded[offset : offset + row_count].astype(jnp.float32) * filters[offset]
        )
    value_cols = value_pre.shape[1]
    key_cols = keys_pre.shape[1]
    inner_rows = (
        jax.nn.silu(filtered[:, :value_cols]).reshape(row_count, head_local, head_dim)
        * step_rows[..., None]
    )
    scan_values = inner_rows.astype(jnp.bfloat16).reshape(
        row_count, group_local, head_ratio, head_dim
    )
    scan_keys = (
        filtered[:, value_cols : value_cols + key_cols]
        .astype(jnp.bfloat16)
        .reshape(row_count, group_local, STATE_SIZE)
    )
    scan_query = (
        filtered[:, value_cols + key_cols :]
        .astype(jnp.bfloat16)
        .reshape(row_count, group_local, STATE_SIZE)
    )
    pieces, summaries = block_terms(
        scan_query,
        scan_keys,
        scan_values,
        log_decay.reshape(row_count, group_local, head_ratio),
        BLOCK,
    )
    summary_fwd, summary_bwd, overall = summaries
    gathered_states = (
        lax.all_gather(summary_fwd[None].astype(jnp.bfloat16), "sp", axis=0, tiled=True).astype(
            jnp.float32
        ),
        lax.all_gather(summary_bwd[None].astype(jnp.bfloat16), "sp", axis=0, tiled=True).astype(
            jnp.float32
        ),
        lax.all_gather(overall[None].astype(jnp.bfloat16), "sp", axis=0, tiled=True).astype(
            jnp.float32
        ),
    )
    incoming_fwd, incoming_bwd = combine_all(gathered_states, lax.axis_index("sp"))
    scan_out = finish_terms(pieces, incoming_fwd, incoming_bwd).reshape(
        row_count, head_local * head_dim
    )
    gated_rows = scan_out * jax.nn.silu(gate_rows.astype(jnp.float32))
    per_head = gated_rows.reshape(row_count, head_local, head_dim)
    state_mix = (
        (
            per_head
            * lax.rsqrt(jnp.mean(per_head * per_head, axis=-1, keepdims=True) + 1e-06)
            * state_gain.reshape(head_local, head_dim)
        )
        .astype(jnp.bfloat16)
        .reshape(row_count, head_local * head_dim)
    )
    query_heads = window_sink.shape[0]
    kv_heads = keys_raw.shape[1] // HEAD_DIM
    kv_width = kv_heads * HEAD_DIM
    positions = lax.axis_index("sp") * row_count + jnp.arange(row_count, dtype=jnp.int32)
    query_rot = rotate_grid(
        query_raw.reshape(row_count, query_heads, HEAD_DIM), positions, GRID_WIDTH
    )
    keys_rot = rotate_grid(keys_raw.reshape(row_count, kv_heads, HEAD_DIM), positions, GRID_WIDTH)
    pair_rows = jnp.concatenate([keys_rot.reshape(row_count, kv_width), values_rows], axis=-1)
    padded_pair = extended(pair_rows, (("sp", 0),), WINDOW)
    keys_pad = padded_pair[:, :kv_width].reshape(-1, kv_heads, HEAD_DIM)
    values_pad = padded_pair[:, kv_width:].reshape(-1, kv_heads, HEAD_DIM)
    window_mix = window_attend(
        query_rot,
        keys_pad,
        values_pad,
        window_sink,
        lax.axis_index("sp") * row_count - WINDOW,
        lax.axis_size("sp") * row_count,
        WINDOW,
    )
    return lax.psum_scatter(
        (
            jnp.dot(state_mix, out_state, preferred_element_type=jnp.float32)
            + jnp.dot(window_mix, out_window, preferred_element_type=jnp.float32)
        ).astype(jnp.bfloat16),
        "tp",
        scatter_dimension=0,
        tiled=True,
    )


def fits(*args):
    tokens, state_value, state_keys, state_rate = args[0], args[3], args[4], args[7]
    window_query, window_keys, window_sink = args[13], args[14], args[16]
    parts = lax.axis_size("fs")
    heads = state_rate.shape[0]
    return (
        parts == 4
        and lax.axis_size("tp") == 2
        and lax.axis_size("sp") > 1
        and tokens.shape[0] % (4 * BLOCK) == 0
        and state_keys.shape[1] == parts * STATE_SIZE
        and state_value.shape[1] == parts * STATE_SIZE
        and heads == 2 * parts
        and window_keys.shape[1] == parts * HEAD_DIM
        and window_query.shape[1] == 2 * parts * HEAD_DIM
        and window_sink.shape[0] == 2 * parts
    )


def fused_kernel(
    count,
    tokens,
    w_value,
    w_keys,
    w_query,
    w_gate,
    w_wkeys,
    w_wvalues,
    w_wquery,
    w_sout,
    w_wout,
    norm_gain,
    step_w,
    rate,
    jumps,
    gain,
    tap_value,
    tap_keys,
    tap_query,
    sink,
    out,
    tbuf,
    xbuf,
    wbuf,
    wob,
    stepx,
    cos_t,
    sin_t,
    jbuf,
    cbuf,
    gbuf,
    stbuf,
    nbuf,
    sabuf,
    sbbuf,
    cumbuf,
    edge,
    sqbuf,
    fin,
    gin,
    fout,
    gout,
    kvbuf,
    qbuf,
    mixs,
    mixr,
    psend,
    pown,
    precv,
    loc_sem,
    z_send,
    z_recv,
    x_send,
    x_recv,
    d_send,
    d_recv,
    j_send,
    j_recv,
    h_send,
    h_recv,
    m_send,
    m_recv,
    o_send,
    o_recv,
    p_send,
    p_recv,
):
    f32, bf16 = jnp.float32, jnp.bfloat16
    me, fs, tp = lax.axis_index("sp"), lax.axis_index("fs"), lax.axis_index("tp")
    rows, width = tokens.shape
    depth = w_value.shape[0]
    half = rows // 2
    quarter = half // 2
    blocks = rows // BLOCK
    lanes = STATE_SIZE
    has = [me > 0, me < count - 1]
    beside = [jnp.maximum(me - 1, 0), jnp.minimum(me + 1, count - 1)]
    peers = [fs, fs + 1 - 2 * (fs % 2), fs + 2 - 4 * (fs // 2), 3 - fs]
    other = 1 - tp

    def to(ref_src, ref_dst, send, recv, axis, index):
        return pltpu.make_async_remote_copy(
            src_ref=ref_src,
            dst_ref=ref_dst,
            send_sem=send,
            recv_sem=recv,
            device_id={axis: index},
            device_id_type=pl.DeviceIdType.MESH,
        )

    own_rows = pl.ds(pl.multiple_of(me * depth, depth), depth)
    loads = [pltpu.make_async_copy(tokens, tbuf, loc_sem.at[0])]
    col = 0
    weight_loads = []
    for index, matrix in enumerate(
        (w_value, w_keys, w_query, w_gate, w_wkeys, w_wvalues, w_wquery)
    ):
        size = matrix.shape[1] // 4
        weight_loads.append(
            pltpu.make_async_copy(
                matrix.at[:, pl.ds(pl.multiple_of(fs * size, size), size)],
                wbuf.at[own_rows, pl.ds(col, size)],
                loc_sem.at[1 + index],
            )
        )
        col += size
    out_loads = []
    first_rows = w_sout.shape[0] // 4
    second_rows = w_wout.shape[0] // 4
    for part in range(4):
        out_loads.append(
            pltpu.make_async_copy(
                w_sout.at[pl.ds(part * first_rows, first_rows)],
                wob.at[me, part, pl.ds(0, first_rows)],
                loc_sem.at[8 + 2 * part],
            )
        )
        out_loads.append(
            pltpu.make_async_copy(
                w_wout.at[pl.ds(part * second_rows, second_rows)],
                wob.at[me, part, pl.ds(first_rows, second_rows)],
                loc_sem.at[9 + 2 * part],
            )
        )
    for load in weight_loads + loads:
        load.start()

    barrier = pltpu.get_barrier_semaphore()
    for side in range(2):
        pl.when(has[side])(
            lambda side=side: pl.semaphore_signal(
                barrier,
                inc=1,
                device_id={"sp": beside[side]},
                device_id_type=pl.DeviceIdType.MESH,
            )
        )
    for k in range(1, 4):
        pl.semaphore_signal(
            barrier, inc=1, device_id={"fs": peers[k]}, device_id_type=pl.DeviceIdType.MESH
        )
    pl.semaphore_signal(
        barrier, inc=1, device_id={"tp": other}, device_id_type=pl.DeviceIdType.MESH
    )
    pl.semaphore_wait(barrier, 4 + jnp.minimum(me, 1) + jnp.minimum(count - 1 - me, 1))

    spans = ((0, 4 * lanes), (4 * lanes, 2 * lanes), (6 * lanes, 2 * lanes))

    def line(piece, hop, side):
        origin = me - hop if side == 1 else me + hop
        origin = jnp.clip(origin, 0, count - 1)
        if piece == 3:
            ref = wob.at[origin, fs]
        else:
            start, size = spans[piece]
            ref = wbuf.at[pl.ds(pl.multiple_of(origin * depth, depth), depth), pl.ds(start, size)]
        slot = (side * 4 + piece) * (count - 1) + hop
        return to(ref, ref, z_send.at[slot], z_recv.at[slot], "sp", beside[side])

    def valid(hop, side):
        return me >= hop if side == 1 else me + hop <= count - 1

    def send_line(piece, hop):
        for side in range(2):
            pl.when(has[side] & valid(hop, side))(
                lambda side=side: line(piece, hop, side).start()
            )

    def take_line(piece, hop, then=None):
        for side in range(2):

            def arrive(side=side):
                line_in(piece, hop, side).wait_recv()
                if hop < count - 1:
                    pl.when(has[side])(lambda: line(piece, hop, side).start())
                if then is not None:
                    then(hop, side)

            pl.when(valid(hop, side))(arrive)

    def line_in(piece, hop, side):
        origin = me - hop if side == 1 else me + hop
        origin = jnp.clip(origin, 0, count - 1)
        if piece == 3:
            ref = wob.at[origin, fs]
        else:
            start, size = spans[piece]
            ref = wbuf.at[pl.ds(pl.multiple_of(origin * depth, depth), depth), pl.ds(start, size)]
        slot = (side * 4 + piece) * (count - 1) + hop - 1
        return to(ref, ref, z_send.at[slot], z_recv.at[slot], "sp", beside[side])

    for load in weight_loads:
        load.wait()
    send_line(0, 0)
    send_line(1, 0)

    loads[0].wait()
    norm_rows = 32

    def norm(index, base):
        at = pl.ds(pl.multiple_of(base + index * norm_rows, norm_rows), norm_rows)
        wide = tbuf[at, :].astype(f32)
        scale = lax.rsqrt(jnp.mean(wide * wide, axis=-1, keepdims=True) + 1e-06)
        xbuf[fs, at, :] = (wide * scale * norm_gain[...]).astype(bf16)
        return base

    lax.fori_loop(0, half // norm_rows, norm, tp * half)
    lax.fori_loop(0, half // norm_rows, norm, other * half)
    own_half = pl.ds(pl.multiple_of(tp * half, half), half)
    x_own = [
        to(
            xbuf.at[fs, own_half],
            xbuf.at[fs, own_half],
            x_send.at[k - 1],
            x_recv.at[k - 1],
            "fs",
            peers[k],
        )
        for k in (1, 2)
    ]
    for copy in x_own:
        copy.start()
    j_own = [
        to(jumps, jbuf.at[fs], j_send.at[k], j_recv.at[k], "fs", peers[k]) for k in range(1, 4)
    ]
    for copy in j_own:
        copy.start()
    for load in out_loads:
        load.start()
    jbuf[fs, :, :] = jumps[...]

    lane = lax.broadcasted_iota(jnp.int32, (1, lanes), 1)
    low = lane < lanes // 2
    q4 = HEAD_DIM // 4

    def table(index, carry):
        at = pl.ds(pl.multiple_of(index * BLOCK, BLOCK), BLOCK)
        spot = lax.broadcasted_iota(jnp.int32, (BLOCK, lanes), 0) + me * rows + index * BLOCK
        place = jnp.where(low, spot // GRID_WIDTH, spot % GRID_WIDTH).astype(f32)
        inverse = jnp.exp((lane % q4).astype(f32) * (-math.log(10000.0) / q4))
        angle = place * inverse
        cos_t[at, :] = jnp.cos(angle)
        sin_t[at, :] = jnp.where(lane % (2 * q4) < q4, -1.0, 1.0) * jnp.sin(angle)
        return carry

    lax.fori_loop(0, blocks, table, 0)
    heads_all = step_w.shape[1]
    first_head = (tp * 4 + fs) * 2
    pick = (
        lax.broadcasted_iota(jnp.int32, (heads_all, lanes), 0)
        == first_head + lax.broadcasted_iota(jnp.int32, (heads_all, lanes), 1) // (lanes // 2)
    )
    stepx[...] = jnp.dot(
        step_w[...], pick.astype(f32).astype(bf16), preferred_element_type=f32
    ).astype(bf16)

    take_line(0, 1)
    send_line(2, 0)

    x_first = pl.ds(pl.multiple_of(tp * half, quarter), quarter)
    x_second = pl.ds(pl.multiple_of(tp * half + quarter, quarter), quarter)

    def x_in(k, at, slot):
        return to(xbuf.at[peers[k], at], xbuf.at[peers[k], at], x_send.at[slot], x_recv.at[slot], "fs", peers[k])

    relay = [
        to(xbuf.at[peers[1], x_first], xbuf.at[peers[1], x_first], x_send.at[2], x_recv.at[2], "fs", peers[2]),
        to(xbuf.at[peers[2], x_second], xbuf.at[peers[2], x_second], x_send.at[3], x_recv.at[3], "fs", peers[1]),
    ]
    across = [
        to(xbuf.at[peers[k], own_half], xbuf.at[peers[k], own_half], d_send.at[k - 1], d_recv.at[k - 1], "tp", other)
        for k in range(1, 4)
    ]
    for k in (1, 2):
        x_in(k, own_half, k - 1).wait_recv()
        relay[k - 1].start()
        across[k - 1].start()
    if count > 2:
        take_line(0, 2)
    take_line(1, 1)
    x_in(3, x_first, 2).wait_recv()
    x_in(3, x_second, 3).wait_recv()
    across[2].start()
    for hop in range(3, count):
        take_line(0, hop)
    other_half = pl.ds(pl.multiple_of(other * half, half), half)
    for k in range(1, 4):
        to(xbuf.at[peers[k], other_half], xbuf.at[peers[k], other_half], d_send.at[k - 1], d_recv.at[k - 1], "tp", other).wait_recv()

    def project_state(index, carry):
        seq, at = index // 2, pl.ds(pl.multiple_of((index % 2) * half, half), half)
        x = xbuf[seq, at, :]
        y = jnp.dot(x, wbuf[:, : 4 * lanes], preferred_element_type=f32)
        to_at = pl.ds(pl.multiple_of((index % 2) * half + 8, 8), half)
        cbuf[seq, to_at, :] = y[:, : 3 * lanes].astype(bf16).astype(f32)
        gbuf[seq, at, :] = y[:, 3 * lanes :].astype(bf16)
        z = jnp.dot(x, stepx[...], preferred_element_type=f32)
        stbuf[seq, at, :] = jnp.maximum(z, 0.0) + jnp.log1p(jnp.exp(-jnp.abs(z)))
        return carry

    lax.fori_loop(0, 8, project_state, 0)
    low_edge, high_edge = pl.ds(0, 8), pl.ds(rows + 8, 8)
    halo = [
        to(cbuf.at[:, pl.ds(8, 8)], cbuf.at[:, high_edge], h_send.at[0], h_recv.at[0], "sp", beside[0]),
        to(cbuf.at[:, pl.ds(rows, 8)], cbuf.at[:, low_edge], h_send.at[1], h_recv.at[1], "sp", beside[1]),
    ]
    halo_in = [
        to(cbuf.at[:, low_edge], cbuf.at[:, low_edge], h_send.at[1], h_recv.at[1], "sp", beside[0]),
        to(cbuf.at[:, high_edge], cbuf.at[:, high_edge], h_send.at[0], h_recv.at[0], "sp", beside[1]),
    ]
    for side in range(2):
        pl.when(has[side])(lambda side=side: halo[side].start())
    edges = (low_edge, high_edge)
    for side in range(2):

        def clear(side=side):
            cbuf[:, edges[side], :] = jnp.zeros((4, 8, 3 * lanes), f32)

        pl.when(jnp.logical_not(has[side]))(clear)
    for hop in range(2, count - 1):
        take_line(1, hop)
    for hop in range(1, count - 1):
        take_line(2, hop)
    for load in out_loads:
        load.wait()
    send_line(3, 0)
    for copy in j_own:
        copy.wait_send()
    for k in range(1, 4):
        to(jumps, jbuf.at[peers[k]], j_send.at[k], j_recv.at[k], "fs", peers[k]).wait_recv()
    for side in range(2):
        pl.when(has[side])(lambda side=side: halo_in[side].wait_recv())

    own_cols = pl.ds(pl.multiple_of(fs * lanes, lanes), lanes)
    taps = jnp.concatenate(
        [ref[:, own_cols].astype(f32) for ref in (tap_value, tap_keys, tap_query)], axis=1
    )
    rate_lane = jnp.where(low, rate[2 * fs], rate[2 * fs + 1])
    row_id = lax.broadcasted_iota(jnp.int32, (BLOCK, lanes), 0)
    col_id = lax.broadcasted_iota(jnp.int32, (BLOCK, lanes), 1)
    lower = (col_id <= row_id).astype(f32)
    left = col_id < lanes // 2
    tap_count = taps.shape[0]
    reach = tap_count // 2
    tall = BLOCK + 16
    high = lax.Precision.HIGHEST

    def scan_block(index, carry):
        seq, blk = index // blocks, index % blocks
        at = pl.ds(pl.multiple_of(blk * BLOCK, BLOCK), BLOCK)
        pre = cbuf[seq, pl.ds(pl.multiple_of(blk * BLOCK, BLOCK), tall), :]
        filt = jnp.zeros((BLOCK, 3 * lanes), f32)
        for tap in range(tap_count):
            moved = pre if tap == reach else pltpu.roll(pre, (reach - tap) % tall, 0)
            filt = filt + moved[8 : 8 + BLOCK] * taps[tap : tap + 1, :]
        fv, fk, fq = filt[:, :lanes], filt[:, lanes : 2 * lanes], filt[:, 2 * lanes :]
        step = stbuf[seq, at, :]
        sv = (fv * jax.nn.sigmoid(fv) * step).astype(bf16)
        sk, sq = fk.astype(bf16), fq.astype(bf16)
        sqbuf[seq, at, :] = sq
        jrows = jbuf[seq, :, at]
        jrow_id = lax.broadcasted_iota(jnp.int32, jrows.shape, 0)
        jrow = [
            jnp.sum(jnp.where(jrow_id == 2 * fs + r, jrows, 0.0), axis=0, keepdims=True)
            for r in range(2)
        ]
        jump = jnp.where(row_id < lanes // 2, jrow[0], jrow[1]).T
        logs = jump - rate_lane * step
        cum = jnp.dot(lower, logs, preferred_element_type=f32, precision=high)
        cumbuf[seq, at, :] = cum
        cum_t = cum.T
        gram = lax.dot_general(sq, sk, (((1,), (1,)), ((), ())), preferred_element_type=f32)
        key_t = sk.astype(f32).T
        near, after, before = [], [], []
        for r in range(2):
            spot = r * (lanes // 2)
            down = cum[:, spot : spot + 1]
            across_row = cum_t[spot : spot + 1, :]
            pair = (gram * jnp.exp(-jnp.abs(down - across_row))).astype(bf16)
            near.append(jnp.dot(pair, sv, preferred_element_type=f32))
            last = across_row[:, BLOCK - 1 : BLOCK]
            k_after = (key_t * jnp.exp(last - across_row)).astype(bf16)
            after.append(jnp.dot(k_after, sv, preferred_element_type=f32))
            k_before = (key_t * jnp.exp(across_row)).astype(bf16)
            before.append(jnp.dot(k_before, sv, preferred_element_type=f32))
        nbuf[seq, at, :] = jnp.where(left, near[0], near[1])
        sabuf[index, :, :] = jnp.where(left, after[0], after[1])
        sbbuf[index, :, :] = jnp.where(left, before[0], before[1])
        return carry

    lax.fori_loop(0, 4 * blocks, scan_block, 0)

    zero_state = jnp.zeros((STATE_SIZE, lanes), f32)

    def total_of(seq, blk):
        return cumbuf[seq, blk * BLOCK + BLOCK - 8 : blk * BLOCK + BLOCK, :][7:8, :]

    def carry_states(seq, carry):
        state, so_far = zero_state, jnp.zeros((1, lanes), f32)
        for blk in range(blocks):
            added = sabuf[seq * blocks + blk, :, :]
            sabuf[seq * blocks + blk, :, :] = state
            edge[seq * blocks + blk, 0:1, :] = so_far
            total = total_of(seq, blk)
            state = state * jnp.exp(total) + added
            so_far = so_far + total
        fout[seq, :, :] = state.astype(bf16)
        edge[4 * blocks + seq, 0:1, :] = so_far
        state, so_far = zero_state, jnp.zeros((1, lanes), f32)
        for blk in range(blocks - 1, -1, -1):
            added = sbbuf[seq * blocks + blk, :, :]
            sbbuf[seq * blocks + blk, :, :] = state
            edge[seq * blocks + blk, 1:2, :] = so_far
            total = total_of(seq, blk)
            state = state * jnp.exp(total) + added
            so_far = so_far + total
        gout[seq, :, :] = state.astype(bf16)
        return carry

    lax.fori_loop(0, 4, carry_states, 0)
    chain = [
        to(gout, gin, h_send.at[2], h_recv.at[2], "sp", beside[0]),
        to(fout, fin, h_send.at[3], h_recv.at[3], "sp", beside[1]),
    ]

    def clear_forward():
        fin[...] = jnp.zeros(fin.shape, bf16)

    def clear_backward():
        gin[...] = jnp.zeros(gin.shape, bf16)

    pl.when(me == 0)(clear_forward)
    pl.when(me == count - 1)(clear_backward)
    pl.when(me == 0)(lambda: chain[1].start())
    pl.when(me == count - 1)(lambda: chain[0].start())

    def rotated(vectors, at):
        lane_full = lax.broadcasted_iota(jnp.int32, vectors.shape, 1)
        turned = jnp.where(
            lane_full % (2 * q4) < q4,
            pltpu.roll(vectors, HEAD_DIM - q4, 1),
            pltpu.roll(vectors, q4, 1),
        )
        return (vectors * cos_t[at, :] + turned * sin_t[at, :]).astype(bf16)

    for hop in range(max(2, count - 1), count):
        take_line(1, hop)

    def project_pair(index, carry):
        seq, at = index // 2, pl.ds(pl.multiple_of((index % 2) * half, half), half)
        y = jnp.dot(
            xbuf[seq, at, :], wbuf[:, 4 * lanes : 6 * lanes], preferred_element_type=f32
        ).astype(bf16)
        to_at = pl.ds(pl.multiple_of((index % 2) * half + WINDOW, WINDOW), half)
        kvbuf[seq, to_at, : HEAD_DIM] = rotated(y[:, :HEAD_DIM].astype(f32), at)
        kvbuf[seq, to_at, HEAD_DIM:] = y[:, HEAD_DIM:]
        return carry

    lax.fori_loop(0, 8, project_pair, 0)
    bottom, top = pl.ds(0, WINDOW), pl.ds(rows + WINDOW, WINDOW)
    kv_edge = [
        to(kvbuf.at[:, pl.ds(WINDOW, WINDOW)], kvbuf.at[:, top], h_send.at[4], h_recv.at[4], "sp", beside[0]),
        to(kvbuf.at[:, pl.ds(rows, WINDOW)], kvbuf.at[:, bottom], h_send.at[5], h_recv.at[5], "sp", beside[1]),
    ]
    kv_in = [
        to(kvbuf.at[:, bottom], kvbuf.at[:, bottom], h_send.at[5], h_recv.at[5], "sp", beside[0]),
        to(kvbuf.at[:, top], kvbuf.at[:, top], h_send.at[4], h_recv.at[4], "sp", beside[1]),
    ]
    for side in range(2):
        pl.when(has[side])(lambda side=side: kv_edge[side].start())
    bands = (bottom, top)
    for side in range(2):

        def clear_band(side=side):
            kvbuf[:, bands[side], :] = jnp.zeros((4, WINDOW, 2 * HEAD_DIM), bf16)

        pl.when(jnp.logical_not(has[side]))(clear_band)

    def forward_step():
        to(fin, fin, h_send.at[3], h_recv.at[3], "sp", beside[0]).wait_recv()

        def add(seq, carry):
            passed = jnp.exp(edge[4 * blocks + seq, 0:1, :])
            fout[seq, :, :] = (
                fout[seq, :, :].astype(f32) + passed * fin[seq, :, :].astype(f32)
            ).astype(bf16)
            return carry

        def pass_on():
            lax.fori_loop(0, 4, add, 0)
            chain[1].start()

        pl.when(has[1])(pass_on)

    def backward_step():
        to(gin, gin, h_send.at[2], h_recv.at[2], "sp", beside[1]).wait_recv()

        def add(seq, carry):
            passed = jnp.exp(edge[4 * blocks + seq, 0:1, :])
            gout[seq, :, :] = (
                gout[seq, :, :].astype(f32) + passed * gin[seq, :, :].astype(f32)
            ).astype(bf16)
            return carry

        def pass_on():
            lax.fori_loop(0, 4, add, 0)
            chain[0].start()

        pl.when(has[0])(pass_on)

    pl.when(has[0])(forward_step)
    pl.when(has[1])(backward_step)

    gain_row = gain[:, own_cols]

    def split_dot(a, b):
        top_bits = b.astype(bf16)
        rest = (b - top_bits.astype(f32)).astype(bf16)
        return jnp.dot(a, top_bits, preferred_element_type=f32) + jnp.dot(
            a, rest, preferred_element_type=f32
        )

    def finish_block(index, carry):
        seq, blk = index // blocks, index % blocks
        at = pl.ds(pl.multiple_of(blk * BLOCK, BLOCK), BLOCK)
        ahead = sabuf[index, :, :] + jnp.exp(edge[index, 0:1, :]) * fin[seq, :, :].astype(f32)
        behind = sbbuf[index, :, :] + jnp.exp(edge[index, 1:2, :]) * gin[seq, :, :].astype(f32)
        sq = sqbuf[seq, at, :]
        cum = cumbuf[seq, at, :]
        total = cum[BLOCK - 1 : BLOCK, :]
        mixed = (
            nbuf[seq, at, :]
            + jnp.exp(cum) * split_dot(sq, ahead)
            + jnp.exp(total - cum) * split_dot(sq, behind)
        )
        g = gbuf[seq, at, :].astype(f32)
        gated = mixed * (g * jax.nn.sigmoid(g))
        square = gated * gated
        first = jnp.sum(jnp.where(left, square, 0.0), axis=-1, keepdims=True)
        second = jnp.sum(jnp.where(left, 0.0, square), axis=-1, keepdims=True)
        mean = jnp.where(left, first, second) * (2.0 / lanes)
        mixs[seq, at, :lanes] = (gated * lax.rsqrt(mean + 1e-06) * gain_row).astype(bf16)
        return carry

    lax.fori_loop(0, 4 * blocks, finish_block, 0)
    state_part, window_part = pl.ds(0, lanes), pl.ds(lanes, 2 * HEAD_DIM)

    def swap(k, part, slot):
        return to(
            mixs.at[peers[k], :, part],
            mixr.at[fs, :, part],
            m_send.at[slot * 4 + k],
            m_recv.at[slot * 4 + k],
            "fs",
            peers[k],
        )

    def swap_in(k, part, slot):
        ref = mixr.at[peers[k], :, part]
        return to(ref, ref, m_send.at[slot * 4 + k], m_recv.at[slot * 4 + k], "fs", peers[k])

    for k in (3, 1, 2):
        swap(k, state_part, 0).start()

    def spread(hop, side):
        origin = jnp.clip(me - hop if side == 1 else me + hop, 0, count - 1)
        for k in (3, 1, 2):
            to(
                wob.at[origin, fs],
                wob.at[origin, fs],
                o_send.at[origin * 4 + k],
                o_recv.at[origin * 4 + k],
                "fs",
                peers[k],
            ).start()

    take_line(3, 1, spread)

    for hop in range(count - 1, count):
        take_line(2, hop)

    def project_query(index, carry):
        seq, at = index // 2, pl.ds(pl.multiple_of((index % 2) * half, half), half)
        y = jnp.dot(
            xbuf[seq, at, :], wbuf[:, 6 * lanes :], preferred_element_type=f32
        ).astype(bf16).astype(f32)
        for r in range(2):
            qbuf[seq, at, r * HEAD_DIM : (r + 1) * HEAD_DIM] = rotated(
                y[:, r * HEAD_DIM : (r + 1) * HEAD_DIM], at
            )
        return carry

    lax.fori_loop(0, 8, project_query, 0)
    for side in range(2):
        pl.when(has[side])(lambda side=side: kv_in[side].wait_recv())
    band = 3 * WINDOW
    q_id = lax.broadcasted_iota(jnp.int32, (2 * WINDOW, band), 0)
    b_id = lax.broadcasted_iota(jnp.int32, (2 * WINDOW, band), 1)
    within = jnp.abs(b_id - WINDOW - q_id % WINDOW) <= WINDOW
    sink_col = jnp.where(
        lax.broadcasted_iota(jnp.int32, (2 * WINDOW, 1), 0) < WINDOW,
        sink[2 * fs],
        sink[2 * fs + 1],
    )

    def attend(seq):
        def body(blk, carry):
            at = pl.ds(pl.multiple_of(blk * WINDOW, WINDOW), WINDOW)
            wide = pl.ds(pl.multiple_of(blk * WINDOW, WINDOW), band)
            q = jnp.concatenate([qbuf[seq, at, :HEAD_DIM], qbuf[seq, at, HEAD_DIM:]], axis=0)
            s = lax.dot_general(
                q,
                kvbuf[seq, wide, :HEAD_DIM],
                (((1,), (1,)), ((), ())),
                preferred_element_type=f32,
            ) * (HEAD_DIM ** (-0.5))
            place = me * rows + (blk - 1) * WINDOW + b_id
            ok = within & (place >= 0) & (place < count * rows)
            s = jnp.where(ok, s, -1e30)
            m = jnp.maximum(jnp.max(s, axis=-1, keepdims=True), sink_col)
            w = jnp.where(ok, jnp.exp(s - m), 0.0)
            total = jnp.exp(sink_col - m) + jnp.sum(w, axis=-1, keepdims=True)
            p = (w * (1.0 / total)).astype(bf16)
            o = jnp.dot(p, kvbuf[seq, wide, HEAD_DIM:], preferred_element_type=f32).astype(bf16)
            mixs[seq, at, lanes : lanes + HEAD_DIM] = o[:WINDOW]
            mixs[seq, at, lanes + HEAD_DIM :] = o[WINDOW:]
            return carry

        lax.fori_loop(0, blocks, body, 0)

    def attend_peer(step, carry):
        seq = jnp.where(step == 0, peers[3], jnp.where(step == 1, peers[1], jnp.where(step == 2, peers[2], fs)))
        attend(seq)
        for index, k in enumerate((3, 1, 2)):
            pl.when(step == index)(lambda k=k: swap(k, window_part, 1).start())
        return carry

    lax.fori_loop(0, 4, attend_peer, 0)
    mixr[fs, :, :] = mixs[fs, :, :]
    for hop in range(2, count - 1):
        take_line(3, hop, spread)
    for k in range(1, 4):
        swap_in(k, state_part, 0).wait_recv()
        swap_in(k, window_part, 1).wait_recv()

    cols = w_sout.shape[1]

    def share(origin, at):
        total = jnp.zeros((half, cols), f32)
        for part in range(4):
            total = total + jnp.dot(
                mixr[part, at, :], wob[origin, part, :, :], preferred_element_type=f32
            )
        return total.astype(bf16)

    def trade(origin):
        return to(
            psend.at[origin], precv.at[origin], p_send.at[origin], p_recv.at[origin], "tp", other
        )

    def out_quarter(step, carry):
        hop, side = (step + 1) // 2, (step + 1) % 2
        origin = me + jnp.where(side == 1, -hop, hop)
        there = (origin >= 0) & (origin < count) & ((hop > 0) | (side == 1))
        origin = jnp.clip(origin, 0, count - 1)

        def work():
            def gather():
                for k in range(1, 4):
                    to(
                        wob.at[origin, peers[k]],
                        wob.at[origin, peers[k]],
                        o_send.at[origin * 4 + k],
                        o_recv.at[origin * 4 + k],
                        "fs",
                        peers[k],
                    ).wait_recv()

            pl.when(hop > 0)(gather)
            psend[origin, :, :] = share(origin, other_half)
            trade(origin).start()
            pown[origin, :, :] = share(origin, own_half)

        pl.when(there)(work)
        return carry

    lax.fori_loop(0, 3, out_quarter, 0)
    if count > 2:
        take_line(3, count - 1, spread)
        lax.fori_loop(3, 2 * count - 1, out_quarter, 0)
    for origin in range(count):
        trade(origin).wait_recv()
        at = pl.ds(origin * cols, cols)
        out[:, at] = (
            pown[origin, :, :].astype(f32) + precv[origin, :, :].astype(f32)
        ).astype(bf16)

    for piece in range(4):
        for hop in range(count - 1):
            for side in range(2):
                pl.when(has[side] & valid(hop, side))(
                    lambda piece=piece, hop=hop, side=side: line(piece, hop, side).wait_send()
                )
    for copy in x_own + relay + across:
        copy.wait_send()
    for side in range(2):
        pl.when(has[side])(lambda side=side: halo[side].wait_send())
        pl.when(has[side])(lambda side=side: chain[side].wait_send())
        pl.when(has[side])(lambda side=side: kv_edge[side].wait_send())
    for k in range(1, 4):
        swap(k, state_part, 0).wait_send()
        swap(k, window_part, 1).wait_send()

        def left_plane(origin, carry, k=k):
            ref = wob.at[origin, fs]
            slot = origin * 4 + k
            pl.when(origin != me)(
                lambda: to(ref, ref, o_send.at[slot], o_recv.at[slot], "fs", peers[k]).wait_send()
            )
            return carry

        lax.fori_loop(0, count, left_plane, 0)
    for origin in range(count):
        trade(origin).wait_send()


def fused_shards(
    tokens,
    norm_gain,
    state_gate,
    state_value,
    state_keys,
    state_query,
    state_step,
    state_rate,
    state_jumps,
    state_gain,
    filter_value,
    filter_keys,
    filter_query,
    window_query,
    window_keys,
    window_values,
    window_sink,
    state_output,
    window_output,
):
    count = lax.axis_size("sp")
    rows, width = tokens.shape
    lanes = STATE_SIZE
    blocks = rows // BLOCK
    depth = state_value.shape[0]
    cols = state_output.shape[1]
    out_rows = (state_output.shape[0] + window_output.shape[0]) // 4
    f32, bf16 = jnp.float32, jnp.bfloat16
    vmem = pltpu.VMEM
    dma = pltpu.SemaphoreType.DMA
    hbm = pl.BlockSpec(memory_space=pl.ANY)
    chip = pl.BlockSpec(memory_space=pltpu.VMEM)
    scalar = pl.BlockSpec(memory_space=pltpu.SMEM)
    jumps = state_jumps.T
    half = rows // 2
    return pl.pallas_call(
        functools.partial(fused_kernel, count),
        out_shape=jax.ShapeDtypeStruct((half, width), bf16),
        in_specs=[hbm] * 10
        + [chip, chip, scalar, chip, chip, chip, chip, chip, scalar],
        out_specs=chip,
        scratch_shapes=[
            vmem((rows, width), bf16),
            vmem((4, rows, width), bf16),
            vmem((count * depth, 8 * lanes), bf16),
            vmem((count, 4, out_rows, cols), bf16),
            vmem((width, lanes), bf16),
            vmem((rows, lanes), f32),
            vmem((rows, lanes), f32),
            vmem((4,) + jumps.shape, f32),
            vmem((4, rows + 16, 3 * lanes), f32),
            vmem((4, rows, lanes), bf16),
            vmem((4, rows, lanes), f32),
            vmem((4, rows, lanes), f32),
            vmem((4 * blocks, STATE_SIZE, lanes), f32),
            vmem((4 * blocks, STATE_SIZE, lanes), f32),
            vmem((4, rows, lanes), f32),
            vmem((4 * blocks + 4, 8, lanes), f32),
            vmem((4, rows, lanes), bf16),
            vmem((4, STATE_SIZE, lanes), bf16),
            vmem((4, STATE_SIZE, lanes), bf16),
            vmem((4, STATE_SIZE, lanes), bf16),
            vmem((4, STATE_SIZE, lanes), bf16),
            vmem((4, rows + 2 * WINDOW, 2 * HEAD_DIM), bf16),
            vmem((4, rows, 2 * HEAD_DIM), bf16),
            vmem((4, rows, 3 * lanes), bf16),
            vmem((4, rows, 3 * lanes), bf16),
            vmem((count, half, cols), bf16),
            vmem((count, half, cols), bf16),
            vmem((count, half, cols), bf16),
            dma((16,)),
            dma((8 * (count - 1),)),
            dma((8 * (count - 1),)),
            dma((4,)),
            dma((4,)),
            dma((3,)),
            dma((3,)),
            dma((4,)),
            dma((4,)),
            dma((6,)),
            dma((6,)),
            dma((8,)),
            dma((8,)),
            dma((4 * count,)),
            dma((4 * count,)),
            dma((count,)),
            dma((count,)),
        ],
        compiler_params=pltpu.CompilerParams(
            collective_id=0, has_side_effects=True, vmem_limit_bytes=62 * 1024 * 1024
        ),
        name="fused_layer",
    )(
        tokens,
        state_value,
        state_keys,
        state_query,
        state_gate,
        window_keys,
        window_values,
        window_query,
        state_output,
        window_output,
        norm_gain.reshape(1, -1),
        state_step,
        state_rate,
        jumps,
        state_gain.reshape(1, -1),
        filter_value,
        filter_keys,
        filter_query,
        window_sink,
    )


def solution(mesh):
    placed = (
        P(("fs", "sp"), None),
        P(),
        P("sp", "tp"),
        P("sp", "tp"),
        P("sp", "tp"),
        P("sp", "tp"),
        P(),
        P("tp"),
        P(("fs", "sp"), "tp"),
        P("tp"),
        P(None, "tp"),
        P(None, "tp"),
        P(None, "tp"),
        P("sp", "tp"),
        P("sp", "tp"),
        P("sp", "tp"),
        P("tp"),
        P("tp", "sp"),
        P("tp", "sp"),
    )
    def plan(*args):
        return (fused_shards if fits(*args) else shards)(*args)

    return jax.shard_map(
        plan, mesh=mesh, in_specs=placed, out_specs=P(("fs", "sp", "tp"), None), check_vma=False
    )
```

profile of v0, /device:TPU:1, one launch (start us, length us, event | category | flops | bytes accessed | tf_op | source)
XLA Modules:
  0.0 177.1 jit_solution(10894228908579232926)
XLA Ops:
  0.0 1.8 %copy.20.step_w = bf16[2048,16]{1,0:T(8,128)(2,1)} copy(bf16[2048,16]{0,1:T(8,128)(2,1)} %param.25) | data formatting | bytes 131072 | tf_op args[6]
  1.8 172.9 %fused_layer.1 = bf16[256,2048]{1,0:T(8,128)(2,1)} custom-call(bf16[512,2048]{1,0:T(8,128)(2,1)} %tokens.1, bf16[512,512]{1,0:T(8,128)(2,1)} %w_value.1, bf16[512,512]{1,0:T(8,128)(2,1)} %w_keys.1, bf16[512,512]{1,0:T(8,128)(2,1)} %w_query.1, bf16[512,512]{1,0:T(8,128)(2,1)} %w_gate.1, bf16[512,512]{1,0:T(8,128)(2,1)} %w_wkeys.1, ...), custom_call_target="tpu_custom_call" | custom-call | tf_op jit(solution)/shard_map/fused_layer/pallas_call | solution.py:1146
  174.8 2.3 %copy.22 = bf16[256,2048]{1,0:T(8,128)(2,1)} copy(bf16[256,2048]{1,0:T(8,128)(2,1)} %fused_layer.1) | data formatting | bytes 2097152
where the time goes:
time: 177 us
  Pallas kernels  173 us (98%)
  local copies, waits for them, and re-layouts  4.15 us (2%)
    pallas_call x1, Pallas kernels, fused_shards(): pl.pallas_call(functools.partial(fused_kernel, count), out_shape=jax.Shap...  173 us
    unnamed x2, local copies, waits for them, and re-layouts  4.15 us

commit v1 on v0

--- a/solution.py
+++ b/solution.py
@@ -406,10 +406,14 @@
     xbuf,
     wbuf,
     wob,
+    stepw,
     stepx,
     cos_t,
     sin_t,
     jbuf,
+    bias,
+    acc,
+    oacc,
     cbuf,
     gbuf,
     stbuf,
@@ -430,6 +434,7 @@
     psend,
     pown,
     precv,
+    sums,
     loc_sem,
     z_send,
     z_recv,
@@ -490,6 +495,7 @@
     out_loads = []
     first_rows = w_sout.shape[0] // 4
     second_rows = w_wout.shape[0] // 4
+    out_rows = first_rows + second_rows
     for part in range(4):
         out_loads.append(
             pltpu.make_async_copy(
@@ -505,7 +511,8 @@
                 loc_sem.at[9 + 2 * part],
             )
         )
-    for load in weight_loads + loads:
+    step_load = pltpu.make_async_copy(step_w, stepw, loc_sem.at[16])
+    for load in weight_loads + loads + [step_load]:
         load.start()
 
     barrier = pltpu.get_barrier_semaphore()
@@ -549,17 +556,26 @@
                 lambda side=side: line(piece, hop, side).start()
             )
 
-    def take_line(piece, hop, then=None):
+    def take_line(piece, hop, then=None, mode=None, hold=False):
         for side in range(2):
+            wanted = valid(hop, side)
+            if mode == "pass":
+                wanted = wanted & has[side]
+            elif mode == "pass_end":
+                wanted = wanted & has[side] & jnp.logical_not(valid(hop + 1, side))
+            elif mode == "pass_rest":
+                wanted = wanted & has[side] & valid(hop + 1, side)
+            elif mode == "keep":
+                wanted = wanted & jnp.logical_not(has[side])
 
             def arrive(side=side):
                 line_in(piece, hop, side).wait_recv()
-                if hop < count - 1:
+                if hop < count - 1 and not hold:
                     pl.when(has[side])(lambda: line(piece, hop, side).start())
                 if then is not None:
                     then(hop, side)
 
-            pl.when(valid(hop, side))(arrive)
+            pl.when(wanted)(arrive)
 
     def line_in(piece, hop, side):
         origin = me - hop if side == 1 else me + hop
@@ -627,18 +643,33 @@
         return carry
 
     lax.fori_loop(0, blocks, table, 0)
+
+    def window_bias(index, carry):
+        q_id = lax.broadcasted_iota(jnp.int32, (2 * WINDOW, 3 * WINDOW), 0)
+        b_id = lax.broadcasted_iota(jnp.int32, (2 * WINDOW, 3 * WINDOW), 1)
+        blk = jnp.where(index == 2, blocks - 1, index)
+        place = me * rows + (blk - 1) * WINDOW + b_id
+        ok = jnp.abs(b_id - WINDOW - q_id % WINDOW) <= WINDOW
+        ok = ok & (place >= 0) & (place < count * rows)
+        bias[index, :, :] = jnp.where(ok, 0.0, -1e30)
+        return carry
+
+    lax.fori_loop(0, 3, window_bias, 0)
     heads_all = step_w.shape[1]
     first_head = (tp * 4 + fs) * 2
     pick = (
         lax.broadcasted_iota(jnp.int32, (heads_all, lanes), 0)
         == first_head + lax.broadcasted_iota(jnp.int32, (heads_all, lanes), 1) // (lanes // 2)
     )
+    step_load.wait()
     stepx[...] = jnp.dot(
-        step_w[...], pick.astype(f32).astype(bf16), preferred_element_type=f32
+        stepw[...], pick.astype(f32).astype(bf16), preferred_element_type=f32
     ).astype(bf16)
 
     take_line(0, 1)
-    send_line(2, 0)
+    for load in out_loads:
+        load.wait()
+    send_line(3, 0)
 
     x_first = pl.ds(pl.multiple_of(tp * half, quarter), quarter)
     x_second = pl.ds(pl.multiple_of(tp * half + quarter, quarter), quarter)
@@ -661,24 +692,80 @@
     if count > 2:
         take_line(0, 2)
     take_line(1, 1)
+    inner = has[0] & has[1]
+
+    out_half = out_rows // 2
+
+    def plane(origin, k, at, slot, target):
+        ref = wob.at[origin, peers[k]] if at is None else wob.at[origin, peers[k], at]
+        slot = origin * 4 + slot
+        return to(ref, ref, o_send.at[slot], o_recv.at[slot], "fs", peers[target])
+
+    halves = (pl.ds(0, out_half), pl.ds(out_half, out_half))
+
+    def spread(hop, side):
+        origin = jnp.clip(me - hop if side == 1 else me + hop, 0, count - 1)
+        plane(origin, 0, None, 1, 1).start()
+        plane(origin, 0, None, 2, 2).start()
+
+    def relay_out(hop):
+        for side in range(2):
+
+            def work(side=side):
+                origin = jnp.clip(me - hop if side == 1 else me + hop, 0, count - 1)
+                plane(origin, 1, None, 1, 1).wait_recv()
+                plane(origin, 1, halves[0], 3, 2).start()
+                plane(origin, 2, None, 2, 2).wait_recv()
+                plane(origin, 2, halves[1], 0, 1).start()
+
+            pl.when(valid(hop, side))(work)
+
+    at_top = jnp.where(me == count - 1, 1, 0)
+    most = (count - 1) * depth
+    most_at = pl.ds(pl.multiple_of(at_top * depth, depth), most)
+    last_at = pl.ds(pl.multiple_of((1 - at_top) * most, depth), depth)
+    other_half = pl.ds(pl.multiple_of(other * half, half), half)
+
+    def sequence(step):
+        return jnp.where(
+            step == 0,
+            peers[0],
+            jnp.where(step == 1, peers[1], jnp.where(step == 2, peers[2], peers[3])),
+        )
+
+    def project_most(index, start):
+        seq, at = sequence(index // 2), pl.ds(pl.multiple_of((index % 2) * half, half), half)
+        acc[seq, at, :] = jnp.dot(
+            xbuf[seq, at, most_at], wbuf[most_at, : 4 * lanes], preferred_element_type=f32
+        )
+        z = jnp.dot(xbuf[seq, at, :], stepx[...], preferred_element_type=f32)
+        stbuf[seq, at, :] = jnp.maximum(z, 0.0) + jnp.log1p(jnp.exp(-jnp.abs(z)))
+        return start
+
+    def half_in(k):
+        ref = xbuf.at[peers[k], other_half]
+        to(ref, ref, d_send.at[k - 1], d_recv.at[k - 1], "tp", other).wait_recv()
+
+    half_in(1)
+    half_in(2)
+    lax.fori_loop(0, 6, project_most, 0)
     x_in(3, x_first, 2).wait_recv()
     x_in(3, x_second, 3).wait_recv()
     across[2].start()
+    take_line(3, 1, spread, hold=True)
+    half_in(3)
+    lax.fori_loop(6, 8, project_most, 0)
     for hop in range(3, count):
         take_line(0, hop)
-    other_half = pl.ds(pl.multiple_of(other * half, half), half)
-    for k in range(1, 4):
-        to(xbuf.at[peers[k], other_half], xbuf.at[peers[k], other_half], d_send.at[k - 1], d_recv.at[k - 1], "tp", other).wait_recv()
 
     def project_state(index, carry):
         seq, at = index // 2, pl.ds(pl.multiple_of((index % 2) * half, half), half)
-        x = xbuf[seq, at, :]
-        y = jnp.dot(x, wbuf[:, : 4 * lanes], preferred_element_type=f32)
+        y = acc[seq, at, :] + jnp.dot(
+            xbuf[seq, at, last_at], wbuf[last_at, : 4 * lanes], preferred_element_type=f32
+        )
         to_at = pl.ds(pl.multiple_of((index % 2) * half + 8, 8), half)
         cbuf[seq, to_at, :] = y[:, : 3 * lanes].astype(bf16).astype(f32)
         gbuf[seq, at, :] = y[:, 3 * lanes :].astype(bf16)
-        z = jnp.dot(x, stepx[...], preferred_element_type=f32)
-        stbuf[seq, at, :] = jnp.maximum(z, 0.0) + jnp.log1p(jnp.exp(-jnp.abs(z)))
         return carry
 
     lax.fori_loop(0, 8, project_state, 0)
@@ -700,13 +787,11 @@
             cbuf[:, edges[side], :] = jnp.zeros((4, 8, 3 * lanes), f32)
 
         pl.when(jnp.logical_not(has[side]))(clear)
+    if count > 2:
+        send_line(3, 1)
     for hop in range(2, count - 1):
-        take_line(1, hop)
-    for hop in range(1, count - 1):
-        take_line(2, hop)
-    for load in out_loads:
-        load.wait()
-    send_line(3, 0)
+        take_line(1, hop, mode="pass")
+    send_line(2, 0)
     for copy in j_own:
         copy.wait_send()
     for k in range(1, 4):
@@ -728,7 +813,7 @@
     tall = BLOCK + 16
     high = lax.Precision.HIGHEST
 
-    def scan_block(index, carry):
+    def scan_block(index):
         seq, blk = index // blocks, index % blocks
         at = pl.ds(pl.multiple_of(blk * BLOCK, BLOCK), BLOCK)
         pre = cbuf[seq, pl.ds(pl.multiple_of(blk * BLOCK, BLOCK), tall), :]
@@ -740,7 +825,6 @@
         step = stbuf[seq, at, :]
         sv = (fv * jax.nn.sigmoid(fv) * step).astype(bf16)
         sk, sq = fk.astype(bf16), fq.astype(bf16)
-        sqbuf[seq, at, :] = sq
         jrows = jbuf[seq, :, at]
         jrow_id = lax.broadcasted_iota(jnp.int32, jrows.shape, 0)
         jrow = [
@@ -750,7 +834,6 @@
         jump = jnp.where(row_id < lanes // 2, jrow[0], jrow[1]).T
         logs = jump - rate_lane * step
         cum = jnp.dot(lower, logs, preferred_element_type=f32, precision=high)
-        cumbuf[seq, at, :] = cum
         cum_t = cum.T
         gram = lax.dot_general(sq, sk, (((1,), (1,)), ((), ())), preferred_element_type=f32)
         key_t = sk.astype(f32).T
@@ -766,12 +849,31 @@
             after.append(jnp.dot(k_after, sv, preferred_element_type=f32))
             k_before = (key_t * jnp.exp(across_row)).astype(bf16)
             before.append(jnp.dot(k_before, sv, preferred_element_type=f32))
-        nbuf[seq, at, :] = jnp.where(left, near[0], near[1])
-        sabuf[index, :, :] = jnp.where(left, after[0], after[1])
-        sbbuf[index, :, :] = jnp.where(left, before[0], before[1])
-        return carry
-
-    lax.fori_loop(0, 4 * blocks, scan_block, 0)
+
+        def store():
+            sqbuf[seq, at, :] = sq
+            cumbuf[seq, at, :] = cum
+            nbuf[seq, at, :] = jnp.where(left, near[0], near[1])
+            sabuf[index, :, :] = jnp.where(left, after[0], after[1])
+            sbbuf[index, :, :] = jnp.where(left, before[0], before[1])
+
+        return store
+
+    def pairs_of(block):
+        def body(index, carry):
+            for store in [block(2 * index + k) for k in range(2)]:
+                store()
+            return carry
+
+        return body
+
+    lax.fori_loop(0, 2 * blocks, pairs_of(scan_block), 0)
+
+    relay_out(1)
+    for hop in range(2, count - 1):
+        take_line(3, hop, spread, hold=True)
+    if count > 2:
+        take_line(2, 1, mode="pass_end")
 
     zero_state = jnp.zeros((STATE_SIZE, lanes), f32)
 
@@ -826,8 +928,8 @@
         )
         return (vectors * cos_t[at, :] + turned * sin_t[at, :]).astype(bf16)
 
-    for hop in range(max(2, count - 1), count):
-        take_line(1, hop)
+    for hop in range(2, count):
+        take_line(1, hop, mode="keep")
 
     def project_pair(index, carry):
         seq, at = index // 2, pl.ds(pl.multiple_of((index % 2) * half, half), half)
@@ -849,8 +951,6 @@
         to(kvbuf.at[:, bottom], kvbuf.at[:, bottom], h_send.at[5], h_recv.at[5], "sp", beside[0]),
         to(kvbuf.at[:, top], kvbuf.at[:, top], h_send.at[4], h_recv.at[4], "sp", beside[1]),
     ]
-    for side in range(2):
-        pl.when(has[side])(lambda side=side: kv_edge[side].start())
     bands = (bottom, top)
     for side in range(2):
 
@@ -891,9 +991,46 @@
 
         pl.when(has[0])(pass_on)
 
-    pl.when(has[0])(forward_step)
-    pl.when(has[1])(backward_step)
-
+    near_first = 2 * me < count
+    pl.when(inner & near_first)(forward_step)
+    pl.when(inner)(backward_step)
+    pl.when(inner & jnp.logical_not(near_first))(forward_step)
+    for hop in range(2, count - 1):
+        send_line(3, hop)
+    if count > 2:
+        take_line(2, 1, mode="pass_rest")
+    for hop in range(2, count - 1):
+        take_line(2, hop, mode="pass")
+    for side in range(2):
+        pl.when(has[side])(lambda side=side: kv_edge[side].start())
+    for hop in range(2, count - 1):
+        relay_out(hop)
+
+    state_part, window_part = pl.ds(0, lanes), pl.ds(lanes, 2 * HEAD_DIM)
+
+    spread_rows = (
+        pl.ds(0, rows),
+        pl.ds(BLOCK, rows - 2 * BLOCK),
+        pl.ds(0, BLOCK),
+        pl.ds(rows - BLOCK, BLOCK),
+    )
+
+    def swap(k, part, slot):
+        return to(
+            mixs.at[peers[k], spread_rows[slot], part],
+            mixr.at[fs, spread_rows[slot], part],
+            m_send.at[slot * 4 + k],
+            m_recv.at[slot * 4 + k],
+            "fs",
+            peers[k],
+        )
+
+    def swap_in(k, part, slot):
+        ref = mixr.at[peers[k], spread_rows[slot], part]
+        return to(ref, ref, m_send.at[slot * 4 + k], m_recv.at[slot * 4 + k], "fs", peers[k])
+
+    pl.when(has[0] & jnp.logical_not(has[1]))(forward_step)
+    pl.when(has[1] & jnp.logical_not(has[0]))(backward_step)
     gain_row = gain[:, own_cols]
 
     def split_dot(a, b):
@@ -903,7 +1040,7 @@
             a, rest, preferred_element_type=f32
         )
 
-    def finish_block(index, carry):
+    def finish_block(index):
         seq, blk = index // blocks, index % blocks
         at = pl.ds(pl.multiple_of(blk * BLOCK, BLOCK), BLOCK)
         ahead = sabuf[index, :, :] + jnp.exp(edge[index, 0:1, :]) * fin[seq, :, :].astype(f32)
@@ -922,51 +1059,41 @@
         first = jnp.sum(jnp.where(left, square, 0.0), axis=-1, keepdims=True)
         second = jnp.sum(jnp.where(left, 0.0, square), axis=-1, keepdims=True)
         mean = jnp.where(left, first, second) * (2.0 / lanes)
-        mixs[seq, at, :lanes] = (gated * lax.rsqrt(mean + 1e-06) * gain_row).astype(bf16)
-        return carry
-
-    lax.fori_loop(0, 4 * blocks, finish_block, 0)
-    state_part, window_part = pl.ds(0, lanes), pl.ds(lanes, 2 * HEAD_DIM)
-
-    def swap(k, part, slot):
-        return to(
-            mixs.at[peers[k], :, part],
-            mixr.at[fs, :, part],
-            m_send.at[slot * 4 + k],
-            m_recv.at[slot * 4 + k],
-            "fs",
-            peers[k],
-        )
-
-    def swap_in(k, part, slot):
-        ref = mixr.at[peers[k], :, part]
-        return to(ref, ref, m_send.at[slot * 4 + k], m_recv.at[slot * 4 + k], "fs", peers[k])
-
+        mix = (gated * lax.rsqrt(mean + 1e-06) * gain_row).astype(bf16)
+
+        def store():
+            mixs[seq, at, :lanes] = mix
+
+        return store
+
+    lax.fori_loop(0, 2 * blocks, pairs_of(finish_block), 0)
     for k in (3, 1, 2):
         swap(k, state_part, 0).start()
 
-    def spread(hop, side):
-        origin = jnp.clip(me - hop if side == 1 else me + hop, 0, count - 1)
-        for k in (3, 1, 2):
-            to(
-                wob.at[origin, fs],
-                wob.at[origin, fs],
-                o_send.at[origin * 4 + k],
-                o_recv.at[origin * 4 + k],
-                "fs",
-                peers[k],
-            ).start()
-
-    take_line(3, 1, spread)
-
-    for hop in range(count - 1, count):
-        take_line(2, hop)
+
+    if count > 2:
+        take_line(3, count - 1, spread)
+
+    def query_most(index, carry):
+        seq, at = index // 2, pl.ds(pl.multiple_of((index % 2) * half, half), half)
+        acc[seq, at, : 2 * HEAD_DIM] = jnp.dot(
+            xbuf[seq, at, most_at], wbuf[most_at, 6 * lanes :], preferred_element_type=f32
+        )
+        return carry
+
+    for hop in range(1, count - 1):
+        take_line(2, hop, mode="keep")
+    lax.fori_loop(0, 8, query_most, 0)
+    if count > 2:
+        relay_out(count - 1)
+    take_line(2, count - 1, mode="keep")
 
     def project_query(index, carry):
         seq, at = index // 2, pl.ds(pl.multiple_of((index % 2) * half, half), half)
-        y = jnp.dot(
-            xbuf[seq, at, :], wbuf[:, 6 * lanes :], preferred_element_type=f32
-        ).astype(bf16).astype(f32)
+        y = acc[seq, at, : 2 * HEAD_DIM] + jnp.dot(
+            xbuf[seq, at, last_at], wbuf[last_at, 6 * lanes :], preferred_element_type=f32
+        )
+        y = y.astype(bf16).astype(f32)
         for r in range(2):
             qbuf[seq, at, r * HEAD_DIM : (r + 1) * HEAD_DIM] = rotated(
                 y[:, r * HEAD_DIM : (r + 1) * HEAD_DIM], at
@@ -974,109 +1101,146 @@
         return carry
 
     lax.fori_loop(0, 8, project_query, 0)
-    for side in range(2):
-        pl.when(has[side])(lambda side=side: kv_in[side].wait_recv())
     band = 3 * WINDOW
-    q_id = lax.broadcasted_iota(jnp.int32, (2 * WINDOW, band), 0)
-    b_id = lax.broadcasted_iota(jnp.int32, (2 * WINDOW, band), 1)
-    within = jnp.abs(b_id - WINDOW - q_id % WINDOW) <= WINDOW
-    sink_col = jnp.where(
+    log2e = math.log2(math.e)
+    sink_col = log2e * jnp.where(
         lax.broadcasted_iota(jnp.int32, (2 * WINDOW, 1), 0) < WINDOW,
         sink[2 * fs],
         sink[2 * fs + 1],
     )
 
-    def attend(seq):
-        def body(blk, carry):
-            at = pl.ds(pl.multiple_of(blk * WINDOW, WINDOW), WINDOW)
-            wide = pl.ds(pl.multiple_of(blk * WINDOW, WINDOW), band)
-            q = jnp.concatenate([qbuf[seq, at, :HEAD_DIM], qbuf[seq, at, HEAD_DIM:]], axis=0)
-            s = lax.dot_general(
-                q,
-                kvbuf[seq, wide, :HEAD_DIM],
-                (((1,), (1,)), ((), ())),
-                preferred_element_type=f32,
-            ) * (HEAD_DIM ** (-0.5))
-            place = me * rows + (blk - 1) * WINDOW + b_id
-            ok = within & (place >= 0) & (place < count * rows)
-            s = jnp.where(ok, s, -1e30)
-            m = jnp.maximum(jnp.max(s, axis=-1, keepdims=True), sink_col)
-            w = jnp.where(ok, jnp.exp(s - m), 0.0)
-            total = jnp.exp(sink_col - m) + jnp.sum(w, axis=-1, keepdims=True)
-            p = (w * (1.0 / total)).astype(bf16)
-            o = jnp.dot(p, kvbuf[seq, wide, HEAD_DIM:], preferred_element_type=f32).astype(bf16)
+    def attend_block(seq, blk):
+        at = pl.ds(pl.multiple_of(blk * WINDOW, WINDOW), WINDOW)
+        wide = pl.ds(pl.multiple_of(blk * WINDOW, WINDOW), band)
+        q = jnp.concatenate([qbuf[seq, at, :HEAD_DIM], qbuf[seq, at, HEAD_DIM:]], axis=0)
+        s = lax.dot_general(
+            q,
+            kvbuf[seq, wide, :HEAD_DIM],
+            (((1,), (1,)), ((), ())),
+            preferred_element_type=f32,
+        )
+        kind = jnp.where(blk == 0, 0, jnp.where(blk == blocks - 1, 2, 1))
+        s = s * (HEAD_DIM ** (-0.5) * log2e) + bias[kind, :, :]
+        m = jnp.maximum(jnp.max(s, axis=-1, keepdims=True), sink_col)
+        w = jnp.exp2(s - m)
+        total = jnp.exp2(sink_col - m) + jnp.sum(w, axis=-1, keepdims=True)
+        p = (w * (1.0 / total)).astype(bf16)
+        o = jnp.dot(p, kvbuf[seq, wide, HEAD_DIM:], preferred_element_type=f32).astype(bf16)
+
+        def store():
             mixs[seq, at, lanes : lanes + HEAD_DIM] = o[:WINDOW]
             mixs[seq, at, lanes + HEAD_DIM :] = o[WINDOW:]
+
+        return store
+
+    def far_first(step):
+        return jnp.where(
+            step == 0,
+            peers[3],
+            jnp.where(step == 1, peers[1], jnp.where(step == 2, peers[2], peers[0])),
+        )
+
+    def attend_inner(step, carry):
+        seq = far_first(step)
+
+        def body(index, carry):
+            for store in [attend_block(seq, 1 + 2 * index + k) for k in range(2)]:
+                store()
             return carry
 
-        lax.fori_loop(0, blocks, body, 0)
-
-    def attend_peer(step, carry):
-        seq = jnp.where(step == 0, peers[3], jnp.where(step == 1, peers[1], jnp.where(step == 2, peers[2], fs)))
-        attend(seq)
+        lax.fori_loop(0, blocks // 2 - 1, body, 0)
         for index, k in enumerate((3, 1, 2)):
             pl.when(step == index)(lambda k=k: swap(k, window_part, 1).start())
         return carry
 
-    lax.fori_loop(0, 4, attend_peer, 0)
-    mixr[fs, :, :] = mixs[fs, :, :]
-    for hop in range(2, count - 1):
-        take_line(3, hop, spread)
-    for k in range(1, 4):
-        swap_in(k, state_part, 0).wait_recv()
-        swap_in(k, window_part, 1).wait_recv()
+    lax.fori_loop(0, 4, attend_inner, 0)
+    for side in range(2):
+        pl.when(has[side])(lambda side=side: kv_in[side].wait_recv())
+
+    def attend_edges(step, carry):
+        seq = far_first(step)
+        for store in [attend_block(seq, blk) for blk in (0, blocks - 1)]:
+            store()
+        for index, k in enumerate((3, 1, 2)):
+
+            def send(k=k):
+                swap(k, window_part, 2).start()
+                swap(k, window_part, 3).start()
+
+            pl.when(step == index)(send)
+        return carry
+
+    lax.fori_loop(0, 4, attend_edges, 0)
 
     cols = w_sout.shape[1]
 
-    def share(origin, at):
-        total = jnp.zeros((half, cols), f32)
-        for part in range(4):
-            total = total + jnp.dot(
-                mixr[part, at, :], wob[origin, part, :, :], preferred_element_type=f32
-            )
-        return total.astype(bf16)
+    def out_in(origin):
+        def work():
+            plane(origin, 3, halves[0], 3, 2).wait_recv()
+            plane(origin, 3, halves[1], 0, 1).wait_recv()
+
+        pl.when(origin != me)(work)
 
     def trade(origin):
         return to(
             psend.at[origin], precv.at[origin], p_send.at[origin], p_recv.at[origin], "tp", other
         )
 
-    def out_quarter(step, carry):
-        hop, side = (step + 1) // 2, (step + 1) % 2
-        origin = me + jnp.where(side == 1, -hop, hop)
-        there = (origin >= 0) & (origin < count) & ((hop > 0) | (side == 1))
-        origin = jnp.clip(origin, 0, count - 1)
-
-        def work():
-            def gather():
-                for k in range(1, 4):
-                    to(
-                        wob.at[origin, peers[k]],
-                        wob.at[origin, peers[k]],
-                        o_send.at[origin * 4 + k],
-                        o_recv.at[origin * 4 + k],
-                        "fs",
-                        peers[k],
-                    ).wait_recv()
-
-            pl.when(hop > 0)(gather)
-            psend[origin, :, :] = share(origin, other_half)
-            trade(origin).start()
-            pown[origin, :, :] = share(origin, own_half)
-
-        pl.when(there)(work)
-        return carry
-
-    lax.fori_loop(0, 3, out_quarter, 0)
-    if count > 2:
-        take_line(3, count - 1, spread)
-        lax.fori_loop(3, 2 * count - 1, out_quarter, 0)
-    for origin in range(count):
+    def product(ref, part, origin, at):
+        return jnp.dot(ref[part, at, :], wob[origin, part, :, :], preferred_element_type=f32)
+
+    def hand_over(origin, totals):
+        psend[origin, :, :] = totals[0].astype(bf16)
+        trade(origin).start()
+        pown[origin, :, :] = totals[1].astype(bf16)
+
+    row_halves = (other_half, own_half)
+
+    def add_part(ref, part, first=False, last=False):
+        def body(index, carry):
+            origin = index
+            if first:
+                out_in(origin)
+            totals = [product(ref, part, origin, at) for at in row_halves]
+            if not first:
+                totals = [x + oacc[origin, at, :] for x, at in zip(totals, row_halves)]
+            if last:
+                hand_over(origin, totals)
+            else:
+                for x, at in zip(totals, row_halves):
+                    oacc[origin, at, :] = x
+            return carry
+
+        lax.fori_loop(0, count, body, 0)
+
+    def store_out(origin):
+        return pltpu.make_async_copy(
+            sums.at[origin],
+            out.at[:, pl.ds(pl.multiple_of(origin * cols, cols), cols)],
+            loc_sem.at[17 + origin],
+        )
+
+    def finish_out(origin):
         trade(origin).wait_recv()
-        at = pl.ds(origin * cols, cols)
-        out[:, at] = (
+        sums[origin, :, :] = (
             pown[origin, :, :].astype(f32) + precv[origin, :, :].astype(f32)
         ).astype(bf16)
+        store_out(origin).start()
+
+    add_part(mixs, fs, first=True)
+    for k in (3, 1, 2):
+        swap_in(k, state_part, 0).wait_recv()
+        for slot in range(1, 4):
+            swap_in(k, window_part, slot).wait_recv()
+        add_part(mixr, peers[k], last=k == 2)
+
+    def finish_each(origin, carry):
+        finish_out(origin)
+        return carry
+
+    lax.fori_loop(0, count, finish_each, 0)
+    for origin in range(count):
+        store_out(origin).wait()
 
     for piece in range(4):
         for hop in range(count - 1):
@@ -1092,17 +1256,20 @@
         pl.when(has[side])(lambda side=side: kv_edge[side].wait_send())
     for k in range(1, 4):
         swap(k, state_part, 0).wait_send()
-        swap(k, window_part, 1).wait_send()
-
-        def left_plane(origin, carry, k=k):
-            ref = wob.at[origin, fs]
-            slot = origin * 4 + k
-            pl.when(origin != me)(
-                lambda: to(ref, ref, o_send.at[slot], o_recv.at[slot], "fs", peers[k]).wait_send()
-            )
-            return carry
-
-        lax.fori_loop(0, count, left_plane, 0)
+        for slot in range(1, 4):
+            swap(k, window_part, slot).wait_send()
+
+    def left_plane(origin, carry):
+        def work():
+            plane(origin, 0, None, 1, 1).wait_send()
+            plane(origin, 0, None, 2, 2).wait_send()
+            plane(origin, 1, halves[0], 3, 2).wait_send()
+            plane(origin, 2, halves[1], 0, 1).wait_send()
+
+        pl.when(origin != me)(work)
+        return carry
+
+    lax.fori_loop(0, count, left_plane, 0)
     for origin in range(count):
         trade(origin).wait_send()
 
@@ -1147,17 +1314,21 @@
         functools.partial(fused_kernel, count),
         out_shape=jax.ShapeDtypeStruct((half, width), bf16),
         in_specs=[hbm] * 10
-        + [chip, chip, scalar, chip, chip, chip, chip, chip, scalar],
-        out_specs=chip,
+        + [chip, hbm, scalar, chip, chip, chip, chip, chip, scalar],
+        out_specs=hbm,
         scratch_shapes=[
             vmem((rows, width), bf16),
             vmem((4, rows, width), bf16),
             vmem((count * depth, 8 * lanes), bf16),
             vmem((count, 4, out_rows, cols), bf16),
+            vmem(state_step.shape, bf16),
             vmem((width, lanes), bf16),
             vmem((rows, lanes), f32),
             vmem((rows, lanes), f32),
             vmem((4,) + jumps.shape, f32),
+            vmem((3, 2 * WINDOW, 3 * WINDOW), f32),
+            vmem((4, rows, 4 * lanes), f32),
+            vmem((count, rows, cols), f32),
             vmem((4, rows + 16, 3 * lanes), f32),
             vmem((4, rows, lanes), bf16),
             vmem((4, rows, lanes), f32),
@@ -1178,7 +1349,8 @@
             vmem((count, half, cols), bf16),
             vmem((count, half, cols), bf16),
             vmem((count, half, cols), bf16),
-            dma((16,)),
+            vmem((count, half, cols), bf16),
+            dma((17 + count,)),
             dma((8 * (count - 1),)),
             dma((8 * (count - 1),)),
             dma((4,)),
@@ -1189,8 +1361,8 @@
             dma((4,)),
             dma((6,)),
             dma((6,)),
-            dma((8,)),
-            dma((8,)),
+            dma((16,)),
+            dma((16,)),
             dma((4 * count,)),
             dma((4 * count,)),
             dma((count,)),

time: 177 us -> 132 us (0.75)
  Pallas kernels: 173 us -> 127 us
    pallas_call x1, Pallas kernels: 173 us -> 127 us  [fused_shards(): pl.pallas_call(functools.partial(fused_kernel, count), out_shape=jax.Shap...]
where the time goes in v1:
time: 132 us
  Pallas kernels  127 us (96%)
  local copies, waits for them, and re-layouts  4.15 us (3%)
    pallas_call x1, Pallas kernels, fused_shards(): pl.pallas_call(functools.partial(fused_kernel, count), out_shape=jax.Shap...  127 us
    unnamed x2, local copies, waits for them, and re-layouts  4.15 us

profile of v1, /device:TPU:1, one launch (start us, length us, event | category | flops | bytes accessed | tf_op | source)
XLA Modules:
  0.0 131.6 jit_solution(13388052554742193687)
XLA Ops:
  0.0 1.8 %copy.20.step_w = bf16[2048,16]{1,0:T(8,128)(2,1)} copy(bf16[2048,16]{0,1:T(8,128)(2,1)} %param.25) | data formatting | bytes 131072 | tf_op args[6]
  1.8 127.5 %fused_layer.1 = bf16[256,2048]{1,0:T(8,128)(2,1)} custom-call(bf16[512,2048]{1,0:T(8,128)(2,1)} %tokens.1, bf16[512,512]{1,0:T(8,128)(2,1)} %w_value.1, bf16[512,512]{1,0:T(8,128)(2,1)} %w_keys.1, bf16[512,512]{1,0:T(8,128)(2,1)} %w_query.1, bf16[512,512]{1,0:T(8,128)(2,1)} %w_gate.1, bf16[512,512]{1,0:T(8,128)(2,1)} %w_wkeys.1, ...), custom_call_target="tpu_custom_call" | custom-call | tf_op jit(solution)/shard_map/fused_layer/pallas_call | solution.py:1313
  129.3 2.3 %copy.22 = bf16[256,2048]{1,0:T(8,128)(2,1)} copy(bf16[256,2048]{1,0:T(8,128)(2,1)} %fused_layer.1) | data formatting | bytes 2097152

commit v2 on v1

--- a/solution.py
+++ b/solution.py
@@ -534,7 +534,13 @@
     )
     pl.semaphore_wait(barrier, 4 + jnp.minimum(me, 1) + jnp.minimum(count - 1 - me, 1))
 
-    spans = ((0, 4 * lanes), (4 * lanes, 2 * lanes), (6 * lanes, 2 * lanes))
+    spans = {
+        0: (0, 4 * lanes),
+        1: (4 * lanes, 2 * lanes),
+        2: (6 * lanes, lanes),
+        4: (7 * lanes, lanes),
+    }
+    pieces = 5
 
     def line(piece, hop, side):
         origin = me - hop if side == 1 else me + hop
@@ -544,15 +550,15 @@
         else:
             start, size = spans[piece]
             ref = wbuf.at[pl.ds(pl.multiple_of(origin * depth, depth), depth), pl.ds(start, size)]
-        slot = (side * 4 + piece) * (count - 1) + hop
+        slot = (side * pieces + piece) * (count - 1) + hop
         return to(ref, ref, z_send.at[slot], z_recv.at[slot], "sp", beside[side])
 
     def valid(hop, side):
         return me >= hop if side == 1 else me + hop <= count - 1
 
-    def send_line(piece, hop):
+    def send_line(piece, hop, where=True):
         for side in range(2):
-            pl.when(has[side] & valid(hop, side))(
+            pl.when(has[side] & valid(hop, side) & where)(
                 lambda side=side: line(piece, hop, side).start()
             )
 
@@ -585,7 +591,7 @@
         else:
             start, size = spans[piece]
             ref = wbuf.at[pl.ds(pl.multiple_of(origin * depth, depth), depth), pl.ds(start, size)]
-        slot = (side * 4 + piece) * (count - 1) + hop - 1
+        slot = (side * pieces + piece) * (count - 1) + hop - 1
         return to(ref, ref, z_send.at[slot], z_recv.at[slot], "sp", beside[side])
 
     for load in weight_loads:
@@ -655,15 +661,16 @@
         return carry
 
     lax.fori_loop(0, 3, window_bias, 0)
-    heads_all = step_w.shape[1]
+    kvbuf[:, :, 2 * HEAD_DIM :] = jnp.ones((4, rows + 2 * WINDOW, HEAD_DIM), bf16)
+    heads_all = step_w.shape[0]
     first_head = (tp * 4 + fs) * 2
     pick = (
-        lax.broadcasted_iota(jnp.int32, (heads_all, lanes), 0)
-        == first_head + lax.broadcasted_iota(jnp.int32, (heads_all, lanes), 1) // (lanes // 2)
+        lax.broadcasted_iota(jnp.int32, (lanes, heads_all), 1)
+        == first_head + lax.broadcasted_iota(jnp.int32, (lanes, heads_all), 0) // (lanes // 2)
     )
     step_load.wait()
     stepx[...] = jnp.dot(
-        stepw[...], pick.astype(f32).astype(bf16), preferred_element_type=f32
+        pick.astype(f32).astype(bf16), stepw[...], preferred_element_type=f32
     ).astype(bf16)
 
     take_line(0, 1)
@@ -738,7 +745,9 @@
         acc[seq, at, :] = jnp.dot(
             xbuf[seq, at, most_at], wbuf[most_at, : 4 * lanes], preferred_element_type=f32
         )
-        z = jnp.dot(xbuf[seq, at, :], stepx[...], preferred_element_type=f32)
+        z = lax.dot_general(
+            xbuf[seq, at, :], stepx[...], (((1,), (1,)), ((), ())), preferred_element_type=f32
+        )
         stbuf[seq, at, :] = jnp.maximum(z, 0.0) + jnp.log1p(jnp.exp(-jnp.abs(z)))
         return start
 
@@ -791,7 +800,8 @@
         send_line(3, 1)
     for hop in range(2, count - 1):
         take_line(1, hop, mode="pass")
-    send_line(2, 0)
+    send_line(2, 0, jnp.logical_not(inner))
+    send_line(4, 0, jnp.logical_not(inner))
     for copy in j_own:
         copy.wait_send()
     for k in range(1, 4):
@@ -871,9 +881,10 @@
 
     relay_out(1)
     for hop in range(2, count - 1):
-        take_line(3, hop, spread, hold=True)
+        take_line(3, hop, spread)
     if count > 2:
         take_line(2, 1, mode="pass_end")
+        take_line(4, 1, mode="pass_end")
 
     zero_state = jnp.zeros((STATE_SIZE, lanes), f32)
 
@@ -919,43 +930,47 @@
     pl.when(me == 0)(lambda: chain[1].start())
     pl.when(me == count - 1)(lambda: chain[0].start())
 
-    def rotated(vectors, at):
+    def rotated(vectors):
         lane_full = lax.broadcasted_iota(jnp.int32, vectors.shape, 1)
         turned = jnp.where(
             lane_full % (2 * q4) < q4,
             pltpu.roll(vectors, HEAD_DIM - q4, 1),
             pltpu.roll(vectors, q4, 1),
         )
-        return (vectors * cos_t[at, :] + turned * sin_t[at, :]).astype(bf16)
+        return (vectors * cos_t[...] + turned * sin_t[...]).astype(bf16)
 
     for hop in range(2, count):
         take_line(1, hop, mode="keep")
 
-    def project_pair(index, carry):
-        seq, at = index // 2, pl.ds(pl.multiple_of((index % 2) * half, half), half)
+    def project_pair(seq, carry):
         y = jnp.dot(
-            xbuf[seq, at, :], wbuf[:, 4 * lanes : 6 * lanes], preferred_element_type=f32
+            xbuf[seq, :, :], wbuf[:, 4 * lanes : 6 * lanes], preferred_element_type=f32
         ).astype(bf16)
-        to_at = pl.ds(pl.multiple_of((index % 2) * half + WINDOW, WINDOW), half)
-        kvbuf[seq, to_at, : HEAD_DIM] = rotated(y[:, :HEAD_DIM].astype(f32), at)
-        kvbuf[seq, to_at, HEAD_DIM:] = y[:, HEAD_DIM:]
+        kvbuf[seq, WINDOW : WINDOW + rows, :HEAD_DIM] = rotated(y[:, :HEAD_DIM].astype(f32))
+        kvbuf[seq, WINDOW : WINDOW + rows, HEAD_DIM : 2 * HEAD_DIM] = y[:, HEAD_DIM:]
         return carry
 
-    lax.fori_loop(0, 8, project_pair, 0)
+    lax.fori_loop(0, 4, project_pair, 0)
     bottom, top = pl.ds(0, WINDOW), pl.ds(rows + WINDOW, WINDOW)
+    pair_cols = pl.ds(0, 2 * HEAD_DIM)
+
+    def kv(at):
+        return kvbuf.at[:, at, pair_cols]
+
+    low_rows, high_rows = pl.ds(WINDOW, WINDOW), pl.ds(rows, WINDOW)
     kv_edge = [
-        to(kvbuf.at[:, pl.ds(WINDOW, WINDOW)], kvbuf.at[:, top], h_send.at[4], h_recv.at[4], "sp", beside[0]),
-        to(kvbuf.at[:, pl.ds(rows, WINDOW)], kvbuf.at[:, bottom], h_send.at[5], h_recv.at[5], "sp", beside[1]),
+        to(kv(low_rows), kv(top), h_send.at[4], h_recv.at[4], "sp", beside[0]),
+        to(kv(high_rows), kv(bottom), h_send.at[5], h_recv.at[5], "sp", beside[1]),
     ]
     kv_in = [
-        to(kvbuf.at[:, bottom], kvbuf.at[:, bottom], h_send.at[5], h_recv.at[5], "sp", beside[0]),
-        to(kvbuf.at[:, top], kvbuf.at[:, top], h_send.at[4], h_recv.at[4], "sp", beside[1]),
+        to(kv(bottom), kv(bottom), h_send.at[5], h_recv.at[5], "sp", beside[0]),
+        to(kv(top), kv(top), h_send.at[4], h_recv.at[4], "sp", beside[1]),
     ]
     bands = (bottom, top)
     for side in range(2):
 
         def clear_band(side=side):
-            kvbuf[:, bands[side], :] = jnp.zeros((4, WINDOW, 2 * HEAD_DIM), bf16)
+            kvbuf[:, bands[side], : 2 * HEAD_DIM] = jnp.zeros((4, WINDOW, 2 * HEAD_DIM), bf16)
 
         pl.when(jnp.logical_not(has[side]))(clear_band)
 
@@ -995,39 +1010,46 @@
     pl.when(inner & near_first)(forward_step)
     pl.when(inner)(backward_step)
     pl.when(inner & jnp.logical_not(near_first))(forward_step)
-    for hop in range(2, count - 1):
-        send_line(3, hop)
+    send_line(2, 0, inner)
     if count > 2:
         take_line(2, 1, mode="pass_rest")
+    send_line(4, 0, inner)
     for hop in range(2, count - 1):
         take_line(2, hop, mode="pass")
+    if count > 2:
+        take_line(4, 1, mode="pass_rest")
+    for hop in range(2, count - 1):
+        take_line(4, hop, mode="pass")
     for side in range(2):
         pl.when(has[side])(lambda side=side: kv_edge[side].start())
     for hop in range(2, count - 1):
         relay_out(hop)
-
-    state_part, window_part = pl.ds(0, lanes), pl.ds(lanes, 2 * HEAD_DIM)
-
-    spread_rows = (
-        pl.ds(0, rows),
-        pl.ds(BLOCK, rows - 2 * BLOCK),
-        pl.ds(0, BLOCK),
-        pl.ds(rows - BLOCK, BLOCK),
-    )
-
-    def swap(k, part, slot):
+    if count > 2:
+        take_line(3, count - 1, spread)
+
+    inner_rows = pl.ds(BLOCK, rows - 2 * BLOCK)
+    parts = (
+        (pl.ds(0, rows), pl.ds(0, lanes)),
+        (inner_rows, pl.ds(lanes, HEAD_DIM)),
+        (inner_rows, pl.ds(lanes + HEAD_DIM, HEAD_DIM)),
+        (pl.ds(0, BLOCK), pl.ds(lanes, 2 * HEAD_DIM)),
+        (pl.ds(rows - BLOCK, BLOCK), pl.ds(lanes, 2 * HEAD_DIM)),
+    )
+
+    def swap(k, part):
+        slot = part * 4 + k
         return to(
-            mixs.at[peers[k], spread_rows[slot], part],
-            mixr.at[fs, spread_rows[slot], part],
-            m_send.at[slot * 4 + k],
-            m_recv.at[slot * 4 + k],
+            mixs.at[(peers[k], *parts[part])],
+            mixr.at[(fs, *parts[part])],
+            m_send.at[slot],
+            m_recv.at[slot],
             "fs",
             peers[k],
         )
 
-    def swap_in(k, part, slot):
-        ref = mixr.at[peers[k], spread_rows[slot], part]
-        return to(ref, ref, m_send.at[slot * 4 + k], m_recv.at[slot * 4 + k], "fs", peers[k])
+    def swap_in(k, part):
+        ref, slot = mixr.at[(peers[k], *parts[part])], part * 4 + k
+        return to(ref, ref, m_send.at[slot], m_recv.at[slot], "fs", peers[k])
 
     pl.when(has[0] & jnp.logical_not(has[1]))(forward_step)
     pl.when(has[1] & jnp.logical_not(has[0]))(backward_step)
@@ -1068,51 +1090,65 @@
 
     lax.fori_loop(0, 2 * blocks, pairs_of(finish_block), 0)
     for k in (3, 1, 2):
-        swap(k, state_part, 0).start()
-
-
-    if count > 2:
-        take_line(3, count - 1, spread)
-
-    def query_most(index, carry):
-        seq, at = index // 2, pl.ds(pl.multiple_of((index % 2) * half, half), half)
-        acc[seq, at, : 2 * HEAD_DIM] = jnp.dot(
-            xbuf[seq, at, most_at], wbuf[most_at, 6 * lanes :], preferred_element_type=f32
-        )
-        return carry
+        swap(k, 0).start()
+
+
+    def query_cols(r):
+        return slice((6 + r) * lanes, (7 + r) * lanes)
+
+    def head_cols(r):
+        return slice(r * HEAD_DIM, (r + 1) * HEAD_DIM)
+
+    near_count = max(1, count // 2)
+    near_at = pl.ds(
+        pl.multiple_of(at_top * (count - near_count) * depth, depth), near_count * depth
+    )
+    far_at = pl.ds(
+        pl.multiple_of((1 - at_top) * near_count * depth, depth), (count - near_count) * depth
+    )
+    query_parts = ((most_at, last_at), (near_at, far_at))
+
+    def query_first(r):
+        at = query_parts[r][0]
+
+        def body(seq, carry):
+            acc[seq, :, head_cols(r)] = jnp.dot(
+                xbuf[seq, :, at], wbuf[at, query_cols(r)], preferred_element_type=f32
+            )
+            return carry
+
+        lax.fori_loop(0, 4, body, 0)
+
+    def query_rest(r):
+        at = query_parts[r][1]
+
+        def body(seq, carry):
+            y = acc[seq, :, head_cols(r)] + jnp.dot(
+                xbuf[seq, :, at], wbuf[at, query_cols(r)], preferred_element_type=f32
+            )
+            qbuf[seq, :, head_cols(r)] = rotated(y.astype(bf16).astype(f32))
+            return carry
+
+        lax.fori_loop(0, 4, body, 0)
 
     for hop in range(1, count - 1):
         take_line(2, hop, mode="keep")
-    lax.fori_loop(0, 8, query_most, 0)
-    if count > 2:
-        relay_out(count - 1)
+    query_first(0)
     take_line(2, count - 1, mode="keep")
-
-    def project_query(index, carry):
-        seq, at = index // 2, pl.ds(pl.multiple_of((index % 2) * half, half), half)
-        y = acc[seq, at, : 2 * HEAD_DIM] + jnp.dot(
-            xbuf[seq, at, last_at], wbuf[last_at, 6 * lanes :], preferred_element_type=f32
-        )
-        y = y.astype(bf16).astype(f32)
-        for r in range(2):
-            qbuf[seq, at, r * HEAD_DIM : (r + 1) * HEAD_DIM] = rotated(
-                y[:, r * HEAD_DIM : (r + 1) * HEAD_DIM], at
-            )
-        return carry
-
-    lax.fori_loop(0, 8, project_query, 0)
+    query_rest(0)
     band = 3 * WINDOW
     log2e = math.log2(math.e)
-    sink_col = log2e * jnp.where(
-        lax.broadcasted_iota(jnp.int32, (2 * WINDOW, 1), 0) < WINDOW,
-        sink[2 * fs],
-        sink[2 * fs + 1],
-    )
-
-    def attend_block(seq, blk):
+    def sink_rows(heads):
+        row = lax.broadcasted_iota(jnp.int32, (len(heads) * WINDOW, 1), 0)
+        first = sink[2 * fs + heads[0]]
+        return log2e * jnp.where(row < WINDOW, first, sink[2 * fs + heads[-1]])
+
+    floors = {heads: sink_rows(heads) for heads in ((0,), (1,), (0, 1))}
+
+    def attend_block(seq, blk, heads):
         at = pl.ds(pl.multiple_of(blk * WINDOW, WINDOW), WINDOW)
         wide = pl.ds(pl.multiple_of(blk * WINDOW, WINDOW), band)
-        q = jnp.concatenate([qbuf[seq, at, :HEAD_DIM], qbuf[seq, at, HEAD_DIM:]], axis=0)
+        q = jnp.concatenate([qbuf[seq, at, head_cols(r)] for r in heads], axis=0)
         s = lax.dot_general(
             q,
             kvbuf[seq, wide, :HEAD_DIM],
@@ -1120,16 +1156,19 @@
             preferred_element_type=f32,
         )
         kind = jnp.where(blk == 0, 0, jnp.where(blk == blocks - 1, 2, 1))
-        s = s * (HEAD_DIM ** (-0.5) * log2e) + bias[kind, :, :]
-        m = jnp.maximum(jnp.max(s, axis=-1, keepdims=True), sink_col)
-        w = jnp.exp2(s - m)
-        total = jnp.exp2(sink_col - m) + jnp.sum(w, axis=-1, keepdims=True)
-        p = (w * (1.0 / total)).astype(bf16)
-        o = jnp.dot(p, kvbuf[seq, wide, HEAD_DIM:], preferred_element_type=f32).astype(bf16)
+        floor = floors[heads]
+        s = s * (HEAD_DIM ** (-0.5) * log2e) + bias[kind, : len(heads) * WINDOW, :]
+        m = jnp.maximum(jnp.max(s, axis=-1, keepdims=True), floor)
+        w = jnp.exp2(s - m).astype(bf16)
+        y = jnp.dot(w, kvbuf[seq, wide, HEAD_DIM:], preferred_element_type=f32)
+        total = jnp.exp2(floor - m) + y[:, HEAD_DIM:]
+        o = (y[:, :HEAD_DIM] / total).astype(bf16)
 
         def store():
-            mixs[seq, at, lanes : lanes + HEAD_DIM] = o[:WINDOW]
-            mixs[seq, at, lanes + HEAD_DIM :] = o[WINDOW:]
+            for index, r in enumerate(heads):
+                mixs[seq, at, lanes + r * HEAD_DIM : lanes + (r + 1) * HEAD_DIM] = o[
+                    index * WINDOW : (index + 1) * WINDOW
+                ]
 
         return store
 
@@ -1140,32 +1179,44 @@
             jnp.where(step == 1, peers[1], jnp.where(step == 2, peers[2], peers[0])),
         )
 
-    def attend_inner(step, carry):
-        seq = far_first(step)
-
-        def body(index, carry):
-            for store in [attend_block(seq, 1 + 2 * index + k) for k in range(2)]:
-                store()
+    def attend_inner(r):
+        def each(step, carry):
+            seq = far_first(step)
+
+            def body(index, carry):
+                for store in [attend_block(seq, 1 + 2 * index + k, (r,)) for k in range(2)]:
+                    store()
+                return carry
+
+            lax.fori_loop(0, blocks // 2 - 1, body, 0)
+            for index, k in enumerate((3, 1, 2)):
+                pl.when(step == index)(lambda k=k: swap(k, 1 + r).start())
             return carry
 
-        lax.fori_loop(0, blocks // 2 - 1, body, 0)
-        for index, k in enumerate((3, 1, 2)):
-            pl.when(step == index)(lambda k=k: swap(k, window_part, 1).start())
-        return carry
-
-    lax.fori_loop(0, 4, attend_inner, 0)
+        lax.fori_loop(0, 4, each, 0)
+
+    attend_inner(0)
+    for hop in range(1, near_count):
+        take_line(4, hop, mode="keep")
+    query_first(1)
+    if count > 2:
+        relay_out(count - 1)
+    for hop in range(near_count, count):
+        take_line(4, hop, mode="keep")
+    query_rest(1)
+    attend_inner(1)
     for side in range(2):
         pl.when(has[side])(lambda side=side: kv_in[side].wait_recv())
 
     def attend_edges(step, carry):
         seq = far_first(step)
-        for store in [attend_block(seq, blk) for blk in (0, blocks - 1)]:
+        for store in [attend_block(seq, blk, (0, 1)) for blk in (0, blocks - 1)]:
             store()
         for index, k in enumerate((3, 1, 2)):
 
             def send(k=k):
-                swap(k, window_part, 2).start()
-                swap(k, window_part, 3).start()
+                swap(k, 3).start()
+                swap(k, 4).start()
 
             pl.when(step == index)(send)
         return carry
@@ -1186,9 +1237,6 @@
             psend.at[origin], precv.at[origin], p_send.at[origin], p_recv.at[origin], "tp", other
         )
 
-    def product(ref, part, origin, at):
-        return jnp.dot(ref[part, at, :], wob[origin, part, :, :], preferred_element_type=f32)
-
     def hand_over(origin, totals):
         psend[origin, :, :] = totals[0].astype(bf16)
         trade(origin).start()
@@ -1196,19 +1244,35 @@
 
     row_halves = (other_half, own_half)
 
-    def add_part(ref, part, first=False, last=False):
-        def body(index, carry):
-            origin = index
-            if first:
-                out_in(origin)
-            totals = [product(ref, part, origin, at) for at in row_halves]
-            if not first:
-                totals = [x + oacc[origin, at, :] for x, at in zip(totals, row_halves)]
+    def first_product(origin, carry):
+        out_in(origin)
+        weights = jnp.concatenate(
+            [wob[origin, fs, :, :]] + [wob[origin, peers[k], :lanes, :] for k in range(1, 4)], axis=0
+        )
+        for at in row_halves:
+            mix = jnp.concatenate(
+                [mixs[fs, at, :]] + [mixr[peers[k], at, :lanes] for k in range(1, 4)], axis=1
+            )
+            oacc[origin, at, :] = jnp.dot(mix, weights, preferred_element_type=f32)
+        return carry
+
+    def add_parts(ks, last):
+        def body(origin, carry):
+            weights = jnp.concatenate([wob[origin, peers[k], lanes:, :] for k in ks], axis=0)
+            totals = [
+                oacc[origin, at, :]
+                + jnp.dot(
+                    jnp.concatenate([mixr[peers[k], at, lanes:] for k in ks], axis=1),
+                    weights,
+                    preferred_element_type=f32,
+                )
+                for at in row_halves
+            ]
             if last:
                 hand_over(origin, totals)
             else:
-                for x, at in zip(totals, row_halves):
-                    oacc[origin, at, :] = x
+                for total, at in zip(totals, row_halves):
+                    oacc[origin, at, :] = total
             return carry
 
         lax.fori_loop(0, count, body, 0)
@@ -1227,12 +1291,14 @@
         ).astype(bf16)
         store_out(origin).start()
 
-    add_part(mixs, fs, first=True)
     for k in (3, 1, 2):
-        swap_in(k, state_part, 0).wait_recv()
-        for slot in range(1, 4):
-            swap_in(k, window_part, slot).wait_recv()
-        add_part(mixr, peers[k], last=k == 2)
+        swap_in(k, 0).wait_recv()
+    lax.fori_loop(0, count, first_product, 0)
+    for ks in ((3,), (1, 2)):
+        for k in ks:
+            for part in range(1, 5):
+                swap_in(k, part).wait_recv()
+        add_parts(ks, 2 in ks)
 
     def finish_each(origin, carry):
         finish_out(origin)
@@ -1242,7 +1308,7 @@
     for origin in range(count):
         store_out(origin).wait()
 
-    for piece in range(4):
+    for piece in range(pieces):
         for hop in range(count - 1):
             for side in range(2):
                 pl.when(has[side] & valid(hop, side))(
@@ -1255,9 +1321,8 @@
         pl.when(has[side])(lambda side=side: chain[side].wait_send())
         pl.when(has[side])(lambda side=side: kv_edge[side].wait_send())
     for k in range(1, 4):
-        swap(k, state_part, 0).wait_send()
-        for slot in range(1, 4):
-            swap(k, window_part, slot).wait_send()
+        for part in range(5):
+            swap(k, part).wait_send()
 
     def left_plane(origin, carry):
         def work():
@@ -1321,8 +1386,8 @@
             vmem((4, rows, width), bf16),
             vmem((count * depth, 8 * lanes), bf16),
             vmem((count, 4, out_rows, cols), bf16),
-            vmem(state_step.shape, bf16),
-            vmem((width, lanes), bf16),
+            vmem(state_step.shape[::-1], bf16),
+            vmem((lanes, width), bf16),
             vmem((rows, lanes), f32),
             vmem((rows, lanes), f32),
             vmem((4,) + jumps.shape, f32),
@@ -1342,7 +1407,7 @@
             vmem((4, STATE_SIZE, lanes), bf16),
             vmem((4, STATE_SIZE, lanes), bf16),
             vmem((4, STATE_SIZE, lanes), bf16),
-            vmem((4, rows + 2 * WINDOW, 2 * HEAD_DIM), bf16),
+            vmem((4, rows + 2 * WINDOW, 3 * HEAD_DIM), bf16),
             vmem((4, rows, 2 * HEAD_DIM), bf16),
             vmem((4, rows, 3 * lanes), bf16),
             vmem((4, rows, 3 * lanes), bf16),
@@ -1351,8 +1416,8 @@
             vmem((count, half, cols), bf16),
             vmem((count, half, cols), bf16),
             dma((17 + count,)),
-            dma((8 * (count - 1),)),
-            dma((8 * (count - 1),)),
+            dma((10 * (count - 1),)),
+            dma((10 * (count - 1),)),
             dma((4,)),
             dma((4,)),
             dma((3,)),
@@ -1361,8 +1426,8 @@
             dma((4,)),
             dma((6,)),
             dma((6,)),
-            dma((16,)),
-            dma((16,)),
+            dma((20,)),
+            dma((20,)),
             dma((4 * count,)),
             dma((4 * count,)),
             dma((count,)),
@@ -1384,7 +1449,7 @@
         state_output,
         window_output,
         norm_gain.reshape(1, -1),
-        state_step,
+        state_step.T,
         state_rate,
         jumps,
         state_gain.reshape(1, -1),

time: 132 us -> 126 us (0.955)
  Pallas kernels: 127 us -> 123 us
  local copies, waits for them, and re-layouts: 4.15 us -> 2.3 us
    pallas_call x1, Pallas kernels: 127 us -> 123 us  [fused_shards(): pl.pallas_call(functools.partial(fused_kernel, count), out_shape=jax.Shap...]
    unnamed x2 -> x1, local copies, waits for them, and re-layouts: 4.15 us -> 2.3 us
where the time goes in v2:
time: 126 us
  Pallas kernels  123 us (98%)
  local copies, waits for them, and re-layouts  2.3 us (2%)
    pallas_call x1, Pallas kernels, fused_shards(): pl.pallas_call(functools.partial(fused_kernel, count), out_shape=jax.Shap...  123 us

profile of v2, /device:TPU:1, one launch (start us, length us, event | category | flops | bytes accessed | tf_op | source)
XLA Modules:
  0.0 125.6 jit_solution(4835853152002389231)
XLA Ops:
  0.0 123.3 %fused_layer.1 = bf16[256,2048]{1,0:T(8,128)(2,1)} custom-call(bf16[512,2048]{1,0:T(8,128)(2,1)} %tokens.1, bf16[512,512]{1,0:T(8,128)(2,1)} %w_value.1, bf16[512,512]{1,0:T(8,128)(2,1)} %w_keys.1, bf16[512,512]{1,0:T(8,128)(2,1)} %w_query.1, bf16[512,512]{1,0:T(8,128)(2,1)} %w_gate.1, bf16[512,512]{1,0:T(8,128)(2,1)} %w_wkeys.1, ...), custom_call_target="tpu_custom_call" | custom-call | tf_op jit(solution)/shard_map/fused_layer/pallas_call | solution.py:1378
  123.3 2.3 %copy.21 = bf16[256,2048]{1,0:T(8,128)(2,1)} copy(bf16[256,2048]{1,0:T(8,128)(2,1)} %fused_layer.1) | data formatting | bytes 2097152

commit v3 on v2

--- a/solution.py
+++ b/solution.py
@@ -392,16 +392,23 @@
     w_wquery,
     w_sout,
     w_wout,
-    norm_gain,
+    norm_gain_in,
     step_w,
     rate,
+    jumps_in,
+    gain_in,
+    tap_value_in,
+    tap_keys_in,
+    tap_query_in,
+    sink,
+    out_own,
+    out_other,
+    norm_gain,
     jumps,
     gain,
     tap_value,
     tap_keys,
     tap_query,
-    sink,
-    out,
     tbuf,
     xbuf,
     wbuf,
@@ -433,8 +440,6 @@
     mixr,
     psend,
     pown,
-    precv,
-    sums,
     loc_sem,
     z_send,
     z_recv,
@@ -512,8 +517,18 @@
             )
         )
     step_load = pltpu.make_async_copy(step_w, stepw, loc_sem.at[16])
-    for load in weight_loads + loads + [step_load]:
-        load.start()
+    small = (
+        (norm_gain_in, norm_gain),
+        (jumps_in, jumps),
+        (gain_in, gain),
+        (tap_value_in, tap_value),
+        (tap_keys_in, tap_keys),
+        (tap_query_in, tap_query),
+    )
+    small_loads = [
+        pltpu.make_async_copy(source, target, loc_sem.at[17 + count + index])
+        for index, (source, target) in enumerate(small)
+    ]
 
     barrier = pltpu.get_barrier_semaphore()
     for side in range(2):
@@ -532,6 +547,8 @@
     pl.semaphore_signal(
         barrier, inc=1, device_id={"tp": other}, device_id_type=pl.DeviceIdType.MESH
     )
+    for load in weight_loads + loads + small_loads + [step_load]:
+        load.start()
     pl.semaphore_wait(barrier, 4 + jnp.minimum(me, 1) + jnp.minimum(count - 1 - me, 1))
 
     spans = {
@@ -599,7 +616,8 @@
     send_line(0, 0)
     send_line(1, 0)
 
-    loads[0].wait()
+    for load in loads + small_loads:
+        load.wait()
     norm_rows = 32
 
     def norm(index, base):
@@ -698,7 +716,6 @@
         across[k - 1].start()
     if count > 2:
         take_line(0, 2)
-    take_line(1, 1)
     inner = has[0] & has[1]
 
     out_half = out_rows // 2
@@ -715,7 +732,7 @@
         plane(origin, 0, None, 1, 1).start()
         plane(origin, 0, None, 2, 2).start()
 
-    def relay_out(hop):
+    def relay_out(hop, where=True):
         for side in range(2):
 
             def work(side=side):
@@ -725,7 +742,7 @@
                 plane(origin, 2, None, 2, 2).wait_recv()
                 plane(origin, 2, halves[1], 0, 1).start()
 
-            pl.when(valid(hop, side))(work)
+            pl.when(valid(hop, side) & where)(work)
 
     at_top = jnp.where(me == count - 1, 1, 0)
     most = (count - 1) * depth
@@ -798,8 +815,7 @@
         pl.when(jnp.logical_not(has[side]))(clear)
     if count > 2:
         send_line(3, 1)
-    for hop in range(2, count - 1):
-        take_line(1, hop, mode="pass")
+    take_line(1, 1)
     send_line(2, 0, jnp.logical_not(inner))
     send_line(4, 0, jnp.logical_not(inner))
     for copy in j_own:
@@ -877,11 +893,15 @@
 
         return body
 
-    lax.fori_loop(0, 2 * blocks, pairs_of(scan_block), 0)
-
-    relay_out(1)
+    relay_out(1, jnp.logical_not(inner))
+    lax.fori_loop(0, blocks, pairs_of(scan_block), 0)
+    for hop in range(2, count - 1):
+        take_line(1, hop, mode="pass")
+    relay_out(1, inner)
     for hop in range(2, count - 1):
         take_line(3, hop, spread)
+    lax.fori_loop(blocks, 2 * blocks, pairs_of(scan_block), 0)
+
     if count > 2:
         take_line(2, 1, mode="pass_end")
         take_line(4, 1, mode="pass_end")
@@ -1028,12 +1048,19 @@
         take_line(3, count - 1, spread)
 
     inner_rows = pl.ds(BLOCK, rows - 2 * BLOCK)
+
+    def edge_block(second):
+        return jnp.where(at_top == 1 - second, blocks - 1, 0)
+
+    def edge_rows(second):
+        return pl.ds(pl.multiple_of(edge_block(second) * BLOCK, BLOCK), BLOCK)
+
     parts = (
         (pl.ds(0, rows), pl.ds(0, lanes)),
         (inner_rows, pl.ds(lanes, HEAD_DIM)),
         (inner_rows, pl.ds(lanes + HEAD_DIM, HEAD_DIM)),
-        (pl.ds(0, BLOCK), pl.ds(lanes, 2 * HEAD_DIM)),
-        (pl.ds(rows - BLOCK, BLOCK), pl.ds(lanes, 2 * HEAD_DIM)),
+        (edge_rows(0), pl.ds(lanes, 2 * HEAD_DIM)),
+        (edge_rows(1), pl.ds(lanes, 2 * HEAD_DIM)),
     )
 
     def swap(k, part):
@@ -1134,6 +1161,8 @@
     for hop in range(1, count - 1):
         take_line(2, hop, mode="keep")
     query_first(0)
+    if count > 2:
+        relay_out(count - 1, tp == 1)
     take_line(2, count - 1, mode="keep")
     query_rest(0)
     band = 3 * WINDOW
@@ -1196,32 +1225,35 @@
         lax.fori_loop(0, 4, each, 0)
 
     attend_inner(0)
+    if count > 2:
+        relay_out(count - 1, tp == 0)
     for hop in range(1, near_count):
         take_line(4, hop, mode="keep")
     query_first(1)
-    if count > 2:
-        relay_out(count - 1)
     for hop in range(near_count, count):
         take_line(4, hop, mode="keep")
     query_rest(1)
     attend_inner(1)
-    for side in range(2):
-        pl.when(has[side])(lambda side=side: kv_in[side].wait_recv())
-
-    def attend_edges(step, carry):
-        seq = far_first(step)
-        for store in [attend_block(seq, blk, (0, 1)) for blk in (0, blocks - 1)]:
-            store()
-        for index, k in enumerate((3, 1, 2)):
-
-            def send(k=k):
-                swap(k, 3).start()
-                swap(k, 4).start()
-
-            pl.when(step == index)(send)
-        return carry
-
-    lax.fori_loop(0, 4, attend_edges, 0)
+    def edges_in(where):
+        for side in range(2):
+            pl.when(has[side] & where)(lambda side=side: kv_in[side].wait_recv())
+
+    def attend_edges(second):
+        def body(index, carry):
+            steps = [2 * index + k for k in range(2)]
+            seqs = [far_first(step) for step in steps]
+            for store in [attend_block(seq, edge_block(second), (0, 1)) for seq in seqs]:
+                store()
+            for step, k in enumerate((3, 1, 2)):
+                pl.when(index == step // 2)(lambda k=k: swap(k, 3 + second).start())
+            return carry
+
+        lax.fori_loop(0, 2, body, 0)
+
+    edges_in(inner)
+    attend_edges(0)
+    edges_in(jnp.logical_not(inner))
+    attend_edges(1)
 
     cols = w_sout.shape[1]
 
@@ -1232,15 +1264,29 @@
 
         pl.when(origin != me)(work)
 
+    def columns(origin):
+        return pl.ds(pl.multiple_of(origin * cols, cols), cols)
+
     def trade(origin):
         return to(
-            psend.at[origin], precv.at[origin], p_send.at[origin], p_recv.at[origin], "tp", other
+            psend.at[origin],
+            out_other.at[:, columns(origin)],
+            p_send.at[origin],
+            p_recv.at[origin],
+            "tp",
+            other,
+        )
+
+    def store_own(origin):
+        return pltpu.make_async_copy(
+            pown.at[origin], out_own.at[:, columns(origin)], loc_sem.at[17 + origin]
         )
 
     def hand_over(origin, totals):
         psend[origin, :, :] = totals[0].astype(bf16)
         trade(origin).start()
         pown[origin, :, :] = totals[1].astype(bf16)
+        store_own(origin).start()
 
     row_halves = (other_half, own_half)
 
@@ -1277,20 +1323,6 @@
 
         lax.fori_loop(0, count, body, 0)
 
-    def store_out(origin):
-        return pltpu.make_async_copy(
-            sums.at[origin],
-            out.at[:, pl.ds(pl.multiple_of(origin * cols, cols), cols)],
-            loc_sem.at[17 + origin],
-        )
-
-    def finish_out(origin):
-        trade(origin).wait_recv()
-        sums[origin, :, :] = (
-            pown[origin, :, :].astype(f32) + precv[origin, :, :].astype(f32)
-        ).astype(bf16)
-        store_out(origin).start()
-
     for k in (3, 1, 2):
         swap_in(k, 0).wait_recv()
     lax.fori_loop(0, count, first_product, 0)
@@ -1300,13 +1332,9 @@
                 swap_in(k, part).wait_recv()
         add_parts(ks, 2 in ks)
 
-    def finish_each(origin, carry):
-        finish_out(origin)
-        return carry
-
-    lax.fori_loop(0, count, finish_each, 0)
     for origin in range(count):
-        store_out(origin).wait()
+        trade(origin).wait_recv()
+        store_own(origin).wait()
 
     for piece in range(pieces):
         for hop in range(count - 1):
@@ -1371,17 +1399,22 @@
     vmem = pltpu.VMEM
     dma = pltpu.SemaphoreType.DMA
     hbm = pl.BlockSpec(memory_space=pl.ANY)
-    chip = pl.BlockSpec(memory_space=pltpu.VMEM)
     scalar = pl.BlockSpec(memory_space=pltpu.SMEM)
     jumps = state_jumps.T
     half = rows // 2
-    return pl.pallas_call(
+    own, others = pl.pallas_call(
         functools.partial(fused_kernel, count),
-        out_shape=jax.ShapeDtypeStruct((half, width), bf16),
+        out_shape=[jax.ShapeDtypeStruct((half, width), bf16)] * 2,
         in_specs=[hbm] * 10
-        + [chip, hbm, scalar, chip, chip, chip, chip, chip, scalar],
-        out_specs=hbm,
+        + [hbm, hbm, scalar, hbm, hbm, hbm, hbm, hbm, scalar],
+        out_specs=[hbm, hbm],
         scratch_shapes=[
+            vmem((1, width), f32),
+            vmem(jumps.shape, f32),
+            vmem((1,) + state_gain.shape, f32),
+            vmem(filter_value.shape, bf16),
+            vmem(filter_keys.shape, bf16),
+            vmem(filter_query.shape, bf16),
             vmem((rows, width), bf16),
             vmem((4, rows, width), bf16),
             vmem((count * depth, 8 * lanes), bf16),
@@ -1413,9 +1446,7 @@
             vmem((4, rows, 3 * lanes), bf16),
             vmem((count, half, cols), bf16),
             vmem((count, half, cols), bf16),
-            vmem((count, half, cols), bf16),
-            vmem((count, half, cols), bf16),
-            dma((17 + count,)),
+            dma((23 + count,)),
             dma((10 * (count - 1),)),
             dma((10 * (count - 1),)),
             dma((4,)),
@@ -1458,6 +1489,7 @@
         filter_query,
         window_sink,
     )
+    return (own.astype(f32) + others.astype(f32)).astype(bf16)
 
 
 def solution(mesh):

time: 126 us -> 125 us (level)
  other arithmetic: 0 us -> 2.91 us
  local copies, waits for them, and re-layouts: 2.3 us -> 0 us
    convert_element_type x0 -> x1, other arithmetic: none -> 2.91 us  [fused_shards(): return (own.astype(f32) + others.astype(f32)).astype(bf16)]
    unnamed x1 -> x0, local copies, waits for them, and re-layouts: 2.3 us -> none
    pallas_call x1, Pallas kernels: 123 us -> 122 us  [fused_shards(): pl.pallas_call(functools.partial(fused_kernel, count), out_shape=[jax.Sha...]
where the time goes in v3:
time: 125 us
  Pallas kernels  122 us (98%)
  other arithmetic  2.91 us (2%)
    pallas_call x1, Pallas kernels, fused_shards(): pl.pallas_call(functools.partial(fused_kernel, count), out_shape=[jax.Sha...  122 us
    convert_element_type x1, other arithmetic, fused_shards(): return (own.astype(f32) + others.astype(f32)).astype(bf16)  2.91 us

profile of v3, /device:TPU:1, one launch (start us, length us, event | category | flops | bytes accessed | tf_op | source)
XLA Modules:
  0.0 124.6 jit_solution(7970733054093073467)
XLA Ops:
  0.0 121.7 %fused_layer.1 = (bf16[256,2048]{1,0:T(8,128)(2,1)}, bf16[256,2048]{1,0:T(8,128)(2,1)}) custom-call(bf16[512,2048]{1,0:T(8,128)(2,1)} %tokens.1, bf16[512,512]{1,0:T(8,128)(2,1)} %w_value.1, bf16[512,512]{1,0:T(8,128)(2,1)} %w_keys.1, bf16[512,512]{1,0:T(8,128)(2,1)} %w_query.1, bf16[512,512]{1,0:T(8,128)(2,1)} %w_gate.1, bf16[512,512]{1,0:T(8,128)(2,1)} %w_wkeys.1, ...), custom_call_target="tpu_custom_call" | custom-call | tf_op jit(solution)/shard_map/fused_layer/pallas_call | solution.py:1405
  121.7 2.9 %add_convert_fusion = bf16[256,2048]{1,0:T(8,128)(2,1)} fusion(bf16[256,2048]{1,0:T(8,128)(2,1)} %get-tuple-element.8, bf16[256,2048]{1,0:T(8,128)(2,1)} %get-tuple-element.7), kind=kLoop, calls=%fused_computation | loop fusion | flops 2097152 | bytes 3145728 | tf_op jit(solution)/shard_map/convert_element_type | solution.py:1492

commit v4 on v3

--- a/solution.py
+++ b/solution.py
@@ -1156,7 +1156,7 @@
             qbuf[seq, :, head_cols(r)] = rotated(y.astype(bf16).astype(f32))
             return carry
 
-        lax.fori_loop(0, 4, body, 0)
+        lax.fori_loop(0, 4, body, 0, unroll=2)
 
     for hop in range(1, count - 1):
         take_line(2, hop, mode="keep")
@@ -1321,11 +1321,11 @@
                     oacc[origin, at, :] = total
             return carry
 
-        lax.fori_loop(0, count, body, 0)
+        lax.fori_loop(0, count, body, 0, unroll=2)
 
     for k in (3, 1, 2):
         swap_in(k, 0).wait_recv()
-    lax.fori_loop(0, count, first_product, 0)
+    lax.fori_loop(0, count, first_product, 0, unroll=2)
     for ks in ((3,), (1, 2)):
         for k in ks:
             for part in range(1, 5):

time: 125 us -> 124 us (level)
  no operation moved by 1% of the time
where the time goes in v4:
time: 124 us
  Pallas kernels  121 us (98%)
  other arithmetic  2.91 us (2%)
    pallas_call x1, Pallas kernels, fused_shards(): pl.pallas_call(functools.partial(fused_kernel, count), out_shape=[jax.Sha...  121 us
    convert_element_type x1, other arithmetic, fused_shards(): return (own.astype(f32) + others.astype(f32)).astype(bf16)  2.91 us

profile of v4, /device:TPU:1, one launch (start us, length us, event | category | flops | bytes accessed | tf_op | source)
XLA Modules:
  0.0 123.7 jit_solution(18422991695576871709)
XLA Ops:
  0.0 120.8 %fused_layer.1 = (bf16[256,2048]{1,0:T(8,128)(2,1)}, bf16[256,2048]{1,0:T(8,128)(2,1)}) custom-call(bf16[512,2048]{1,0:T(8,128)(2,1)} %tokens.1, bf16[512,512]{1,0:T(8,128)(2,1)} %w_value.1, bf16[512,512]{1,0:T(8,128)(2,1)} %w_keys.1, bf16[512,512]{1,0:T(8,128)(2,1)} %w_query.1, bf16[512,512]{1,0:T(8,128)(2,1)} %w_gate.1, bf16[512,512]{1,0:T(8,128)(2,1)} %w_wkeys.1, ...), custom_call_target="tpu_custom_call" | custom-call | tf_op jit(solution)/shard_map/fused_layer/pallas_call | solution.py:1405
  120.8 2.9 %add_convert_fusion = bf16[256,2048]{1,0:T(8,128)(2,1)} fusion(bf16[256,2048]{1,0:T(8,128)(2,1)} %get-tuple-element.8, bf16[256,2048]{1,0:T(8,128)(2,1)} %get-tuple-element.7), kind=kLoop, calls=%fused_computation | loop fusion | flops 2097152 | bytes 3145728 | tf_op jit(solution)/shard_map/convert_element_type | solution.py:1492
